TPU v7x, 512 devices: a 4x2x32 block of a 4x8x32 slice. The times are simulated.
512 devices in a mesh: grp: 2 (over y), fs: 64 (over z, core), tp: 4 (over x).
Axes of the slice: x: 4, y: 2, z: 32, core: 2. Of those that a mesh axis runs over, the one named last changes fastest.
The devices are a block of a 4x8x32 slice.
Arguments:
- tokens: bfloat16 [1536, 2048], P(('grp', 'tp')), parts along dimension 0, may hold values from -6 to 6
- routes: int32 [1536, 2], P(('grp', 'tp')), parts along dimension 0, may hold values from 0 to 3, all different within a row; in each aligned block of 192 rows (0 to 191, 192 to 383, ...) at most 128 rows name the same one
- route_weight: float32 [1536, 2], P(('grp', 'tp')), parts along dimension 0, may hold values from 0.2 to 1
- norm_gain: float32 [2048], P('fs'), may hold values from 0.1 to 1.9
- gate_train: float32 [4, 2048, 5632], P('tp', 'fs'), may hold values from -0.125 to 0.125
- up_train: float32 [4, 2048, 5632], P('tp', 'fs'), may hold values from -0.125 to 0.125
- down_train: float32 [4, 5632, 2048], P('tp', None, 'fs'), may hold values from -0.21875 to 0.21875
Outputs:
- gate_serve: bfloat16 [8, 2048, 11264], P(('grp', 'tp'), None, 'fs'), parts along dimension 0
- up_serve: bfloat16 [8, 2048, 11264], P(('grp', 'tp'), None, 'fs'), parts along dimension 0
- down_serve: bfloat16 [8, 11264, 2048], P(('grp', 'tp'), 'fs'), parts along dimension 0
- mixed: bfloat16 [1536, 2048], P(('grp', 'tp'), 'fs'), parts along dimension 0
There are 2 independent parts, one for each index of `grp`. A program takes and returns all parts, laid end to end along the dimension named above; an argument that names none is the same for every part. Nothing has to cross between parts.
Inputs may be any that keep to these rules, and one draw needn't show every extreme that they name: `routes`: each row names 2 different experts. In each aligned block of 192 rows no expert is named by more than 128 rows, a bound that some block reaches.
All inputs are finite; a program needn't handle non-finite values.
Results may differ from a plain program's by a relative error of at most 0.0087.
Values may be sent and summed in bfloat16 or wider, within the bound.
A program may use at most 64 MiB of HBM per device.

v0:
```python
import jax
import jax.numpy as jnp
from jax import lax
from jax.sharding import Mesh
from jax.sharding import PartitionSpec as P

EXPERTS = 4
CAP = 128
FS = ("fs_0", "fs_1")


def cut_along(x, dim, length):
    shape = x.shape
    pieces = x.reshape(*shape[:dim], length, shape[dim] // length, *shape[dim + 1 :])
    return jnp.moveaxis(pieces, dim, 0)


def joined_along(pieces, dim):
    shape = list(pieces.shape[1:])
    shape[dim] *= pieces.shape[0]
    return jnp.moveaxis(pieces, 0, dim).reshape(shape)


def turned_blocks(pieces, axes, turns):
    shape = [lax.axis_size(a) for a in axes]
    pieces = pieces.reshape(*shape, *pieces.shape[1:])
    for k in turns:
        pieces = lax.all_to_all(pieces, axes[k], split_axis=k, concat_axis=k, tiled=True)
    return pieces.reshape(-1, *pieces.shape[len(axes) :])


def exchange_by_chip(x, groups, turns, split_dim, concat_dim):
    length = lax.axis_size(groups[0]) * lax.axis_size(groups[1])
    pieces = cut_along(x, split_dim, length)
    return joined_along(turned_blocks(pieces, groups, turns), concat_dim)


def gather_in_order(x, axes, turns):
    pieces = x
    for k in turns:
        pieces = lax.all_gather(pieces, axes[k])
    done = turns[::-1]
    back = [done.index(k) for k in range(len(axes))]
    pieces = pieces.transpose(*back, *range(len(axes), pieces.ndim))
    return pieces.reshape(-1, *x.shape)


def gather_axes(x, axes, turns, dim):
    return joined_along(gather_in_order(x, axes, turns), dim)


def shards(tokens, routes, route_weight, norm_gain, gate_train, up_train, down_train):
    fs_count = lax.axis_size(FS)
    pieces = min(fs_count, 32)
    copies = fs_count // pieces
    gain_column = norm_gain[:, None]
    gate_low = (gate_train[0] * gain_column).astype(jnp.bfloat16)
    up_low = (up_train[0] * gain_column).astype(jnp.bfloat16)
    down_low = down_train[0].astype(jnp.bfloat16)
    gate_wide = jnp.tile(gate_low, (1, copies))
    up_wide = jnp.tile(up_low, (1, copies))
    down_wide = jnp.tile(down_low, (copies, 1))
    gate_new, up_new = (
        exchange_by_chip(gate_wide, ("fs_0", "fs_1"), (1, 0), 1, 0),
        exchange_by_chip(up_wide, ("fs_0", "fs_1"), (1, 0), 1, 0),
    )
    down_new = lax.all_to_all(down_wide, FS, split_axis=0, concat_axis=1, tiled=True)
    units = gate_new.shape[1]
    tok_float = tokens.astype(jnp.float32)
    normed = (
        tok_float * lax.rsqrt(jnp.mean(tok_float * tok_float, axis=-1, keepdims=True) + 1e-06)
    ).astype(jnp.bfloat16)
    chosen = routes.reshape(-1)
    chosen_hot = (chosen[:, None] == jnp.arange(EXPERTS, dtype=jnp.int32)[None, :]).astype(
        jnp.int32
    )
    before = jnp.cumsum(chosen_hot, axis=0) - chosen_hot
    slot_rank = jnp.sum(before * chosen_hot, axis=1)
    slot_index = (chosen * CAP + slot_rank).reshape(routes.shape)
    slot_range = jnp.arange(EXPERTS * CAP, dtype=jnp.int32)
    select_rows = jnp.any(slot_range[:, None, None] == slot_index[None, :, :], axis=-1).astype(
        jnp.bfloat16
    )
    outgoing = jnp.dot(select_rows, normed, preferred_element_type=jnp.float32).astype(jnp.bfloat16)
    outgoing = outgoing.reshape(EXPERTS, CAP, normed.shape[1])
    arrived = lax.all_to_all(outgoing, "tp", split_axis=0, concat_axis=0, tiled=True).reshape(
        EXPERTS * CAP, normed.shape[1]
    )
    slot_count = EXPERTS * CAP // copies
    copy_index = lax.axis_index(FS) // pieces
    my_rows = lax.dynamic_slice_in_dim(arrived, copy_index * slot_count, slot_count, 0)
    gated = jnp.dot(my_rows, gate_new, preferred_element_type=jnp.float32)
    lifted = jnp.dot(my_rows, up_new, preferred_element_type=jnp.float32)
    hidden = (jax.nn.silu(gated) * lifted).astype(jnp.bfloat16)
    empty = jnp.zeros((EXPERTS * CAP, down_low.shape[1]), jnp.float32)
    piece = gather_axes(hidden[None], FS, (0, 1), 0)

    def one_block(position, running):
        source_copy = position // pieces
        source_block = position % pieces
        block_hidden = lax.dynamic_index_in_dim(piece, position, 0, keepdims=False)
        down_rows = lax.dynamic_slice_in_dim(down_low, source_block * units, units, 0)
        contrib = jnp.dot(block_hidden, down_rows, preferred_element_type=jnp.float32)
        current = lax.dynamic_slice_in_dim(running, source_copy * slot_count, slot_count, 0)
        return lax.dynamic_update_slice_in_dim(
            running, current + contrib, source_copy * slot_count, 0
        )

    expert_out = lax.fori_loop(0, piece.shape[0], one_block, empty).astype(jnp.bfloat16)
    returned = lax.all_to_all(
        expert_out.reshape(EXPERTS, CAP, expert_out.shape[1]),
        "tp",
        split_axis=0,
        concat_axis=0,
        tiled=True,
    )
    returned = returned.reshape(EXPERTS * CAP, expert_out.shape[1]).astype(jnp.float32)
    blend_weight = jnp.sum(
        jnp.where(
            slot_range[None, None, :] == slot_index[:, :, None], route_weight[:, :, None], 0.0
        ),
        axis=1,
    )
    mixed = jnp.dot(blend_weight, returned, preferred_element_type=jnp.float32)
    return (gate_new[None], up_new[None], down_new[None], mixed.astype(jnp.bfloat16))


def solution(mesh):
    split = Mesh(
        mesh.devices.reshape(mesh.shape["grp"], 32, 2, mesh.shape["tp"]),
        ("grp", "fs_0", "fs_1", "tp"),
    )
    placed = (
        P(("grp", "tp"), None),
        P(("grp", "tp"), None),
        P(("grp", "tp"), None),
        P(FS),
        P("tp", FS, None),
        P("tp", FS, None),
        P("tp", None, FS),
    )
    return jax.shard_map(
        shards,
        mesh=split,
        in_specs=placed,
        out_specs=(
            P(("grp", "tp"), None, FS),
            P(("grp", "tp"), None, FS),
            P(("grp", "tp"), FS, None),
            P(("grp", "tp"), FS),
        ),
        check_vma=False,
    )
```

profile of v0, /device:TPU:41, one launch (start us, length us, event | category | flops | bytes accessed | tf_op | source)
XLA Modules:
  0.0 628.6 jit_solution(5880605770526879189)
XLA Ops:
  9.1 2.1 tile.11
  13.4 4.2 all-to-all-start
  20.7 2.1 tile.26
  24.6 2.2 convolution_convert_fusion
  26.8 5.0 all_to_all.46
  31.8 4.3 all-to-all-start.5
  36.1 2.3 copy.106
  38.4 23.5 %all-to-all-done.5 = bf16[4,128,2048]{2,1,0:T(8,128)(2,1)S(1)} async-done(((bf16[4,128,2048]{2,1,0:T(8,128)(2,1)}), bf16[4,128,2048]{2,1,0:T(8,128)(2,1)S(1)}, u32[]{:S(2)}, u32[]{:S(2)}) %all-to-all-start.5) | async-done | bytes 2097184 | tf_op jit(solution)/shard_map/all_to_all | solution.py:86
  61.9 45.5 %all-to-all-start.1 = ((bf16[32,2,32,176]{3,2,1,0:T(8,128)(2,1)}), bf16[32,2,32,176]{3,2,1,0:T(8,128)(2,1)S(1)}, u32[]{:S(2)}, u32[]{:S(2)}) async-start(bf16[32,2,32,176]{3,2,1,0:T(8,128)(2,1)} %copy.106), calls=%async_computation.1 | async-start | bytes 2097152 | tf_op jit(solution)/shard_map/all_to_all | solution.py:28
  107.4 2.3 copy.108
  109.7 102.4 %all-to-all-done.1 = bf16[32,2,32,176]{3,2,1,0:T(8,128)(2,1)S(1)} async-done(((bf16[32,2,32,176]{3,2,1,0:T(8,128)(2,1)}), bf16[32,2,32,176]{3,2,1,0:T(8,128)(2,1)S(1)}, u32[]{:S(2)}, u32[]{:S(2)}) %all-to-all-start.1) | async-done | bytes 720928 | tf_op jit(solution)/shard_map/all_to_all | solution.py:28
  212.1 8.0 %all-to-all-start.3 = ((bf16[32,2,32,176]{3,2,1,0:T(8,128)(2,1)}), bf16[32,2,32,176]{3,2,1,0:T(8,128)(2,1)}, u32[]{:S(2)}, u32[]{:S(2)}) async-start(bf16[32,2,32,176]{3,2,1,0:T(8,128)(2,1)} %copy.108), calls=%async_computation.3 | async-start | bytes 2097152 | tf_op jit(solution)/shard_map/all_to_all | solution.py:28
  220.7 103.9 %all-to-all-done.3 = bf16[32,2,32,176]{3,2,1,0:T(8,128)(2,1)} async-done(((bf16[32,2,32,176]{3,2,1,0:T(8,128)(2,1)}), bf16[32,2,32,176]{3,2,1,0:T(8,128)(2,1)}, u32[]{:S(2)}, u32[]{:S(2)}) %all-to-all-start.3) | async-done | bytes 720928 | tf_op jit(solution)/shard_map/all_to_all | solution.py:28
  324.6 2.4 fusion.7
  327.3 105.9 %all-gather.5.cloned.1.call-done = bf16[8192,176]{0,1:T(8,128)(2,1)} async-done(((bf16[256,176]{0,1:T(8,128)(2,1)}), bf16[8192,176]{0,1:T(8,128)(2,1)}) %all-gather.5.cloned.1.call-update) | async-done | bytes 2883600 | tf_op jit(solution)/shard_map/all_gather | solution.py:41
  433.2 4.3 copy.124
  441.2 3.3 all_to_all.34
  446.1 37.3 %all-to-all-start.4 = ((bf16[64,176,32]{1,2,0:T(8,128)(2,1)}), bf16[64,176,32]{1,2,0:T(8,128)(2,1)S(1)}, u32[]{:S(2)}, u32[]{:S(2)}) async-start(bf16[64,176,32]{1,2,0:T(8,128)(2,1)} %copy.111), calls=%async_computation.4 | async-start | bytes 2097152 | tf_op jit(solution)/shard_map/all_to_all | solution.py:67
  483.4 4.1 all-gather.7.cloned.1.call-done
  487.5 12.9 %copy.115 = bf16[2,32,1,256,176]{4,3,0,1,2:T(8,128)(2,1)} copy(bf16[2,32,1,256,176]{3,1,0,4,2:T(8,128)(2,1)} %bitcast.83) | data formatting | bytes 11534336 | tf_op jit(solution)/shard_map/all_gather | solution.py:41
  501.1 109.7 %while.15 = (s32[]{:T(128)}, f32[512,32]{0,1:T(8,128)}, bf16[64,256,176]{2,1,0:T(8,128)(2,1)}, bf16[5632,32]{1,0:T(8,128)(2,1)S(1)}, s32[]{:T(128)}, /*index=5*/...) while((s32[]{:T(128)}, f32[512,32]{0,1:T(8,128)}, ...), condition=%wide.region_7.8_spmd, body=%wide.region_6.7_spmd.sunk | while | flops 2891798 | bytes 242524 | solution.py:109
  504.5 1.7 fusion.34
  518.2 1.7 fusion.34
  531.9 1.7 fusion.34
  545.6 1.7 fusion.34
  552.5 1.7 fusion.34
  566.2 1.7 fusion.34
  579.9 1.7 fusion.34
  593.6 1.7 fusion.34
  607.3 1.7 fusion.34
  612.2 4.0 all-to-all-start.6
  617.6 2.2 copy.119
  (107 shorter events, 114.8 us)
Async XLA Ops:
  11.8 5.8 copy-start.4
  11.8 8.3 %copy-start.1 = (bf16[192,2048]{1,0:T(8,128)(2,1)S(1)}, bf16[192,2048]{1,0:T(8,128)(2,1)}, u32[]{:S(2)}) copy-start(bf16[192,2048]{1,0:T(8,128)(2,1)} %param.9) | copy-start | bytes 2359300
  13.4 13.4 %all-to-all-start = ((bf16[32,2,32,176]{3,2,0,1:T(8,128)(2,1)}), bf16[32,2,32,176]{3,2,0,1:T(8,128)(2,1)S(1)}, u32[]{:S(2)}, u32[]{:S(2)}) async-start(bf16[32,2,32,176]{3,2,0,1:T(8,128)(2,1)} %copy.105), calls=%async_computation | async-start | bytes 2097152 | tf_op jit(solution)/shard_map/all_to_all | solution.py:28
  23.5 1.1 copy-start.2
  26.8 5.0 copy-start
  31.8 30.1 %all-to-all-start.5 = ((bf16[4,128,2048]{2,1,0:T(8,128)(2,1)}), bf16[4,128,2048]{2,1,0:T(8,128)(2,1)S(1)}, u32[]{:S(2)}, u32[]{:S(2)}) async-start(bf16[4,128,2048]{2,1,0:T(8,128)(2,1)} %bitcast.11), calls=%async_computation.5 | async-start | bytes 4194304 | tf_op jit(solution)/shard_map/all_to_all | solution.py:86
  61.9 150.2 %all-to-all-start.1 = ((bf16[32,2,32,176]{3,2,1,0:T(8,128)(2,1)}), bf16[32,2,32,176]{3,2,1,0:T(8,128)(2,1)S(1)}, u32[]{:S(2)}, u32[]{:S(2)}) async-start(bf16[32,2,32,176]{3,2,1,0:T(8,128)(2,1)} %copy.106), calls=%async_computation.1 | async-start | bytes 2097152 | tf_op jit(solution)/shard_map/all_to_all | solution.py:28
  212.1 112.5 %all-to-all-start.3 = ((bf16[32,2,32,176]{3,2,1,0:T(8,128)(2,1)}), bf16[32,2,32,176]{3,2,1,0:T(8,128)(2,1)}, u32[]{:S(2)}, u32[]{:S(2)}) async-start(bf16[32,2,32,176]{3,2,1,0:T(8,128)(2,1)} %copy.108), calls=%async_computation.3 | async-start | bytes 2097152 | tf_op jit(solution)/shard_map/all_to_all | solution.py:28
  220.0 213.1 %all-gather.5.cloned.1.call-start = ((), (), s32[]{:S(2)}) async-start(), calls=%async_computation.7 | async-start | bytes 2973696 | tf_op jit(solution)/shard_map/all_gather | solution.py:41
  327.1 160.5 %all-gather.7.cloned.1.call-start = ((), (), s32[]{:S(2)}) async-start(), calls=%async_computation.8 | async-start | bytes 8650752 | tf_op jit(solution)/shard_map/all_gather | solution.py:41
  437.4 1.1 copy-start.3
  446.1 166.1 %all-to-all-start.4 = ((bf16[64,176,32]{1,2,0:T(8,128)(2,1)}), bf16[64,176,32]{1,2,0:T(8,128)(2,1)S(1)}, u32[]{:S(2)}, u32[]{:S(2)}) async-start(bf16[64,176,32]{1,2,0:T(8,128)(2,1)} %copy.111), calls=%async_computation.4 | async-start | bytes 2097152 | tf_op jit(solution)/shard_map/all_to_all | solution.py:67
  487.5 128.7 %copy-start.5 = (f32[192,2]{0,1:T(2,128)S(1)}, f32[192,2]{0,1:T(2,128)}, u32[]{:S(2)}) copy-start(f32[192,2]{0,1:T(2,128)} %param.11) | copy-start | bytes 4612
  612.2 8.8 %all-to-all-start.6 = ((bf16[4,128,32]{1,2,0:T(8,128)(2,1)}), bf16[4,128,32]{1,2,0:T(8,128)(2,1)S(1)}, u32[]{:S(2)}, u32[]{:S(2)}) async-start(bf16[4,128,32]{1,2,0:T(8,128)(2,1)} %copy_bitcast_fusion), calls=%async_computation.6 | async-start | bytes 65536 | tf_op jit(solution)/shard_map/all_to_all | solution.py:110
Sparse Core Ops, SparseCore 0:
  327.2 105.9 all-gather.4
  437.6 49.8 all-gather.6
where the time goes:
time: 634 us; the launch traced here: 629 us
  waiting for transfers between devices  340 us (54%)
  matrix products  116 us (18%)
  starting transfers between devices  103 us (16%)
  local copies, waits for them, and re-layouts  45.3 us (7%)
  between operations  14.3 us (2%)
    all_to_all x3, waiting for transfers between devices, turned_blocks(): lax.all_to_all(pieces, axes[k], split_axis=k, concat_axis=k, tiled=True)  206 us
    all_gather x2, waiting for transfers between devices, gather_in_order(): pieces = lax.all_gather(pieces, axes[k])  110 us
    dot_general x64, matrix products, one_block(): jnp.dot(block_hidden, down_rows, preferred_element_type=jnp.float32)  110 us
    all_to_all x3, starting transfers between devices, turned_blocks(): lax.all_to_all(pieces, axes[k], split_axis=k, concat_axis=k, tiled=True)  57.6 us
    all_to_all x1, starting transfers between devices, shards(): lax.all_to_all(down_wide, FS, split_axis=0, concat_axis=1, tiled=True)  37.3 us
    all_to_all x1, waiting for transfers between devices, shards(): lax.all_to_all(outgoing, 'tp', split_axis=0, concat_axis=0, tiled=True)  23.5 us
    all_gather x1, local copies, waits for them, and re-layouts, gather_in_order(): pieces = lax.all_gather(pieces, axes[k])  12.9 us
  transfers between devices with their start and end apart: 8, of which 5 were waited for; matrix products, arithmetic and copies ran while one was open for 23% of the time, Pallas kernels for 0%

commit v1 on v0

v1 whole, which is shorter than its diff:
```python
import functools

import jax
import jax.numpy as jnp
from jax import lax
from jax.experimental import pallas as pl
from jax.experimental.pallas import tpu as pltpu
from jax.sharding import Mesh
from jax.sharding import PartitionSpec as P

EXPERTS = 4
CAP = 128
FS = ("fs_0", "fs_1")
MESH = pl.DeviceIdType.MESH
LANES = 128


def exchange_kernel(
    groups,
    chips,
    gate,
    up,
    down,
    gate_out,
    up_out,
    down_out,
    rows_buf,
    tile_buf,
    quad_send,
    quad_recv,
    ring_send,
    unit_recv,
    group_send,
):
    g = lax.axis_index("grp")
    z = lax.axis_index("fs_0")
    c = lax.axis_index("fs_1")
    quads = chips // 2
    half_ring = chips // 2
    rows, hidden = gate.shape
    units = gate_out.shape[0]
    spread = groups // 2
    share = hidden // 4
    blocks = share // units
    own_count = quads // groups
    q = z // 2
    odd = lax.rem(z, 2)
    me = 2 * odd + c
    half = lax.rem(g + q // spread, 2)
    active = lax.rem(q, spread) == g // 2
    my_block = 2 * lax.rem(z, half_ring) + c
    my_half = my_block // (2 * blocks)
    my_source_core = lax.rem(my_block, 2 * blocks) // blocks
    parity = lax.rem(my_half + g, 2)
    own = jnp.logical_and(active, jnp.logical_and(half == my_half, c == my_source_core))
    inputs = (gate, up, down)
    outputs = (gate_out, up_out, down_out)

    def at(chip, core):
        return {"fs_0": chip, "fs_1": core}

    def own_quad(j):
        return spread * (2 * j + parity) + g // 2

    def sender_of(other):
        right = lax.rem(z - (2 * other + 1) + chips, chips) < half_ring
        return 2 * other + jnp.where(right, 1, 0)

    def target(i):
        chip = half * blocks + c * (blocks // 2) + i // 2
        right = lax.rem(chip - z + 2 * chips, half_ring)
        left = lax.rem(z - chip + 2 * chips, half_ring)
        chip = jnp.where(odd == 1, z + right, z - left + chips)
        return lax.rem(chip, chips), lax.rem(i, 2)

    def place(index):
        return pl.ds(pl.multiple_of(index * LANES, LANES), LANES)

    quad_mates = ((z + 1 - 2 * odd, c), (z, 1 - c), (z + 1 - 2 * odd, 1 - c))

    barrier = pltpu.get_barrier_semaphore()

    @pl.when(active)
    def _():
        for chip, core in quad_mates:
            pl.semaphore_signal(barrier, inc=1, device_id=at(chip, core), device_id_type=MESH)

    def greet(j, _):
        other = own_quad(j)
        chip = sender_of(other)

        @pl.when(jnp.logical_not(jnp.logical_and(own, other == q)))
        def _():
            pl.semaphore_signal(
                barrier, inc=1, device_id=at(chip, my_source_core), device_id_type=MESH
            )

        return 0

    lax.fori_loop(0, own_count, greet, 0)
    for step in range(1, groups):
        pl.semaphore_signal(
            barrier, inc=1, device_id={"grp": lax.rem(g + step, groups)}, device_id_type=MESH
        )
    expected = jnp.where(active, 3 + blocks - jnp.where(own, 1, 0), 0) + groups - 1
    pl.semaphore_wait(barrier, expected)

    def lanes_for(core):
        return pl.ds(pl.multiple_of((2 * half + core) * share, LANES), share)

    def rows_at(index):
        return pl.ds(pl.multiple_of(index * rows, rows), rows)

    def mate_copy(m, k):
        chip, core = quad_mates[k]
        return pltpu.make_async_remote_copy(
            src_ref=inputs[m].at[:, lanes_for(core)],
            dst_ref=rows_buf.at[m, rows_at(me), :],
            send_sem=quad_send.at[m, k],
            recv_sem=quad_recv.at[m, me],
            device_id=at(chip, core),
            device_id_type=MESH,
        )

    def own_copy(m):
        return pltpu.make_async_copy(
            inputs[m].at[:, lanes_for(c)], rows_buf.at[m, rows_at(me), :], quad_recv.at[m, me]
        )

    def ring_copy(m, i):
        chip, core = target(i)
        return pltpu.make_async_remote_copy(
            src_ref=tile_buf.at[m, pl.ds(pl.multiple_of(i * units, 16), units), :],
            dst_ref=outputs[m].at[:, place(q)],
            send_sem=ring_send.at[m, i],
            recv_sem=unit_recv.at[m, q],
            device_id=at(chip, core),
            device_id_type=MESH,
        )

    def group_copy(m, j, step):
        other = own_quad(j)
        return pltpu.make_async_remote_copy(
            src_ref=outputs[m].at[:, place(other)],
            dst_ref=outputs[m].at[:, place(other)],
            send_sem=group_send.at[m, j, step - 1],
            recv_sem=unit_recv.at[m, other],
            device_id={"grp": lax.rem(g + step, groups)},
            device_id_type=MESH,
        )

    def unit_arrival(m, index):
        return pltpu.make_async_remote_copy(
            src_ref=outputs[m].at[:, place(index)],
            dst_ref=outputs[m].at[:, place(index)],
            send_sem=group_send.at[m, 0, 0],
            recv_sem=unit_recv.at[m, index],
            device_id={"grp": lax.rem(g + 1, groups)},
            device_id_type=MESH,
        )

    def is_mine(i):
        chip, core = target(i)
        return jnp.logical_and(chip == z, core == c)

    @pl.when(active)
    def _():
        for m in range(3):
            own_copy(m).start()
            for k in range(3):
                mate_copy(m, k).start()
        for m in range(3):
            own_copy(m).wait()
            for k in range(3):
                chip_back, core_back = quad_mates[k]
                source = 2 * lax.rem(chip_back, 2) + core_back
                pltpu.make_async_remote_copy(
                    src_ref=inputs[m].at[:, lanes_for(c)],
                    dst_ref=rows_buf.at[m, rows_at(source), :],
                    send_sem=quad_send.at[m, k],
                    recv_sem=quad_recv.at[m, source],
                    device_id=at(chip_back, core_back),
                    device_id_type=MESH,
                ).wait_recv()
            tile_buf[m, :, :] = rows_buf[m, :, :].T

            def send(i, _):
                mine = is_mine(i)

                @pl.when(mine)
                def _():
                    outputs[m][:, place(q)] = tile_buf[
                        m, pl.ds(pl.multiple_of(i * units, 16), units), :
                    ]

                @pl.when(jnp.logical_not(mine))
                def _():
                    ring_copy(m, i).start()

                return 0

            lax.fori_loop(0, blocks, send, 0)

    for m in range(3):

        def forward(j, _):
            other = own_quad(j)

            @pl.when(jnp.logical_not(jnp.logical_and(own, other == q)))
            def _():
                unit_arrival(m, other).wait_recv()

            for step in range(1, groups):
                group_copy(m, j, step).start()
            return 0

        lax.fori_loop(0, own_count, forward, 0)

    for m in range(3):

        def arrive(index, _):
            here = jnp.logical_and(
                lax.rem(index, spread) == g // 2, lax.rem(index // spread, 2) == parity
            )

            @pl.when(jnp.logical_not(here))
            def _():
                unit_arrival(m, index).wait_recv()

            return 0

        lax.fori_loop(0, quads, arrive, 0)

    for m in range(3):

        @pl.when(active)
        def _():
            for k in range(3):
                mate_copy(m, k).wait_send()

            def sent(i, _):
                @pl.when(jnp.logical_not(is_mine(i)))
                def _():
                    ring_copy(m, i).wait_send()

                return 0

            lax.fori_loop(0, blocks, sent, 0)

        def passed(j, _):
            for step in range(1, groups):
                group_copy(m, j, step).wait_send()
            return 0

        lax.fori_loop(0, own_count, passed, 0)


def exchange(groups, chips, gate_low, up_low, down_low):
    rows, hidden = gate_low.shape
    units = hidden // chips
    width = rows * 2 * chips
    quads = chips // 2
    share = hidden // 4
    served = jax.ShapeDtypeStruct((units, width), jnp.bfloat16)
    return pl.pallas_call(
        functools.partial(exchange_kernel, groups, chips),
        out_shape=(served, served, served),
        in_specs=[pl.BlockSpec(memory_space=pl.ANY)] * 3,
        out_specs=[pl.BlockSpec(memory_space=pltpu.VMEM)] * 3,
        scratch_shapes=[
            pltpu.VMEM((3, 4 * rows, share), jnp.bfloat16),
            pltpu.VMEM((3, share, 4 * rows), jnp.bfloat16),
            pltpu.SemaphoreType.DMA((3, 3)),
            pltpu.SemaphoreType.DMA((3, 4)),
            pltpu.SemaphoreType.DMA((3, share // units)),
            pltpu.SemaphoreType.DMA((3, quads)),
            pltpu.SemaphoreType.DMA((3, quads // groups, groups - 1)),
        ],
        compiler_params=pltpu.CompilerParams(collective_id=0, has_side_effects=True),
        name="exchange",
    )(gate_low, up_low, down_low)


def shards(tokens, routes, route_weight, norm_gain, gate_train, up_train, down_train):
    fs_count = lax.axis_size(FS)
    chips = lax.axis_size("fs_0")
    groups = lax.axis_size("grp")
    pieces = chips
    copies = fs_count // pieces
    gain_column = norm_gain[:, None]
    gate_low = (gate_train[0] * gain_column).astype(jnp.bfloat16)
    up_low = (up_train[0] * gain_column).astype(jnp.bfloat16)
    down_low = down_train[0].T.astype(jnp.bfloat16)
    gate_new, up_new, down_new = exchange(groups, chips, gate_low, up_low, down_low)
    tok_float = tokens.astype(jnp.float32)
    normed = (
        tok_float * lax.rsqrt(jnp.mean(tok_float * tok_float, axis=-1, keepdims=True) + 1e-06)
    ).astype(jnp.bfloat16)
    chosen = routes.reshape(-1)
    chosen_hot = (chosen[:, None] == jnp.arange(EXPERTS, dtype=jnp.int32)[None, :]).astype(
        jnp.int32
    )
    before = jnp.cumsum(chosen_hot, axis=0) - chosen_hot
    slot_rank = jnp.sum(before * chosen_hot, axis=1)
    slot_index = (chosen * CAP + slot_rank).reshape(routes.shape)
    slot_range = jnp.arange(EXPERTS * CAP, dtype=jnp.int32)
    select_rows = jnp.any(slot_range[:, None, None] == slot_index[None, :, :], axis=-1).astype(
        jnp.bfloat16
    )
    outgoing = jnp.dot(select_rows, normed, preferred_element_type=jnp.float32).astype(jnp.bfloat16)
    outgoing = outgoing.reshape(EXPERTS, CAP, normed.shape[1])
    arrived = lax.all_to_all(outgoing, "tp", split_axis=0, concat_axis=0, tiled=True).reshape(
        EXPERTS * CAP, normed.shape[1]
    )
    slot_count = EXPERTS * CAP // copies
    copy_index = lax.axis_index(FS) // pieces
    my_rows = lax.dynamic_slice_in_dim(arrived, copy_index * slot_count, slot_count, 0)
    dims = (((1,), (1,)), ((), ()))
    gated = lax.dot_general(gate_new, my_rows, dims, preferred_element_type=jnp.float32)
    lifted = lax.dot_general(up_new, my_rows, dims, preferred_element_type=jnp.float32)
    hidden = (jax.nn.silu(gated) * lifted).astype(jnp.bfloat16)
    every = lax.all_gather(hidden, FS)
    every = every.reshape(copies, pieces * hidden.shape[0], slot_count)
    expert_out = jnp.einsum(
        "cu,kus->kcs", down_low, every, preferred_element_type=jnp.float32
    ).astype(jnp.bfloat16)
    columns = expert_out.shape[1]
    back = jnp.moveaxis(expert_out.reshape(copies, columns, EXPERTS // copies, CAP), 2, 1)
    returned = lax.all_to_all(
        back.reshape(EXPERTS, columns, CAP), "tp", split_axis=0, concat_axis=0, tiled=True
    )
    blend_weight = jnp.sum(
        jnp.where(
            slot_range[None, None, :] == slot_index[:, :, None], route_weight[:, :, None], 0.0
        ),
        axis=1,
    ).reshape(-1, EXPERTS, CAP)
    mixed = jnp.einsum(
        "tes,ecs->tc",
        blend_weight,
        returned.astype(jnp.float32),
        preferred_element_type=jnp.float32,
    )
    return (gate_new.T[None], up_new.T[None], down_new[None], mixed.astype(jnp.bfloat16))


def solution(mesh):
    cores = 2
    split = Mesh(
        mesh.devices.reshape(
            mesh.shape["grp"], mesh.shape["fs"] // cores, cores, mesh.shape["tp"]
        ),
        ("grp", "fs_0", "fs_1", "tp"),
    )
    placed = (
        P(("grp", "tp"), None),
        P(("grp", "tp"), None),
        P(("grp", "tp"), None),
        P(FS),
        P("tp", FS, None),
        P("tp", FS, None),
        P("tp", None, FS),
    )
    return jax.shard_map(
        shards,
        mesh=split,
        in_specs=placed,
        out_specs=(
            P(("grp", "tp"), None, FS),
            P(("grp", "tp"), None, FS),
            P(("grp", "tp"), FS, None),
            P(("grp", "tp"), FS),
        ),
        check_vma=False,
    )
```

time: 634 us -> 346 us (0.55)
  waiting for transfers between devices: 340 us -> 152 us
  Pallas kernels: 0 us -> 147 us
  matrix products: 116 us -> 11.7 us
  starting transfers between devices: 103 us -> 8.43 us
  local copies, waits for them, and re-layouts: 45.3 us -> 4.13 us
    all_to_all x5 -> x1, waiting for transfers between devices: 206 us -> 4.12 us  [shards(): lax.all_to_all(back.reshape(EXPERTS, columns, CAP), 'tp', split_axis=0, c...]
    pallas_call x0 -> x1, Pallas kernels: none -> 147 us  [exchange(): pl.pallas_call(functools.partial(exchange_kernel, groups, chips), out_sha...]
    dot_general x67 -> x4, matrix products: 113 us -> 8.44 us  [the longest x1 3.78 us: shards(): jnp.einsum('cu,kus->kcs', down_low, every, preferred_element_type=jnp.flo...]
    all_to_all x5 -> x1, starting transfers between devices: 98.9 us -> 3.99 us  [shards(): lax.all_to_all(back.reshape(EXPERTS, columns, CAP), 'tp', split_axis=0, c...]
    all_gather x2 -> x1, waiting for transfers between devices: 110 us -> 147 us  [shards(): every = lax.all_gather(hidden, FS)]
    all_to_all x1, waiting for transfers between devices: 23.5 us -> 0.01 us  [shards(): lax.all_to_all(outgoing, 'tp', split_axis=0, concat_axis=0, tiled=True)]
    all_gather x1 -> x0, local copies, waits for them, and re-layouts: 12.9 us -> none  [gather_in_order(): pieces = lax.all_gather(pieces, axes[k])]
    all_to_all x4 -> x0, local copies, waits for them, and re-layouts: 9.51 us -> none  [the longest x2 4.91 us: shards(): lax.all_to_all(down_wide, FS, split_axis=0, concat_axis=1, tiled=True)]
  transfers between devices with their start and end apart: 8 -> 3, of which waited for: 5 -> 2; matrix products, arithmetic and copies ran while one was open for 23% -> 1% of each run, Pallas kernels for 0% -> 43%
where the time goes in v1:
time: 346 us; the launch traced here: 344 us
  waiting for transfers between devices  152 us (44%)
  Pallas kernels  147 us (42%)
  between operations  14.1 us (4%)
  matrix products  11.7 us (3%)
  starting transfers between devices  8.43 us (2%)
  other arithmetic  7.4 us (2%)
  local copies, waits for them, and re-layouts  4.13 us (1%)
    all_gather x1, waiting for transfers between devices, shards(): every = lax.all_gather(hidden, FS)  147 us
    pallas_call x1, Pallas kernels, exchange(): pl.pallas_call(functools.partial(exchange_kernel, groups, chips), out_sha...  147 us
  transfers between devices with their start and end apart: 3, of which 2 were waited for; matrix products, arithmetic and copies ran while one was open for 1% of the time, Pallas kernels for 43%

profile of v1, /device:TPU:41, one launch (start us, length us, event | category | flops | bytes accessed | tf_op | source)
XLA Modules:
  0.0 344.2 jit_solution(1912751431827236924)
XLA Ops:
  7.2 0.8 copy.27
  8.0 0.1 eq.56
  8.1 0.1 eq.52
  8.3 1.2 reduce-window.6
  9.5 0.2 slice_reduce_fusion
  9.7 0.2 reduce-window.9
  9.9 0.1 add_bitcast_fusion
  10.0 0.1 reduce_sum.30
  10.2 0.1 copy.29
  10.2 0.7 multiply_add_fusion
  10.9 0.1 fusion.10
  11.1 1.4 fusion
  12.5 3.3 convolution_convert_fusion
  15.8 4.4 %all-to-all-start = ((bf16[4,128,2048]{2,1,0:T(8,128)(2,1)}), bf16[4,128,2048]{2,1,0:T(8,128)(2,1)S(1)}, u32[]{:S(2)}, u32[]{:S(2)}) async-start(bf16[4,128,2048]{2,1,0:T(8,128)(2,1)} %bitcast.10), calls=%async_computation | async-start | bytes 4194304 | tf_op jit(solution)/shard_map/all_to_all | solution.py:312
  20.2 0.8 convert_bitcast_fusion.down
  21.0 2.1 fusion.11
  23.1 146.8 %exchange.1 = (bf16[176,2048]{1,0:T(8,128)(2,1)}, bf16[176,2048]{1,0:T(8,128)(2,1)}, bf16[176,2048]{1,0:T(8,128)(2,1)}) custom-call(bf16[32,5632]{1,0:T(8,128)(2,1)} %get-tuple-element.13.gate, bf16[32,5632]{1,0:T(8,128)(2,1)} %get-tuple-element.12.up, bf16[32,5632]{1,0:T(8,128)(2,1)} %convert_bitcast_fusion.down), custom_call_target="tpu_custom_call" | custom-call | tf_op jit(solution)/shard_map/exchange/pallas_call | solution.py:265
  169.9 0.0 all-to-all-done
  169.9 1.6 fusion.6
  171.5 2.3 fusion.2
  173.8 0.1 all-gather.3.cloned.1.call-update
  173.9 147.3 %all-gather.3.cloned.1.call-done = bf16[11264,256]{1,0:T(8,128)(2,1)} async-done(((bf16[176,256]{1,0:T(8,128)(2,1)}), bf16[11264,256]{1,0:T(8,128)(2,1)}) %all-gather.3.cloned.1.call-update) | async-done | bytes 5767184 | tf_op jit(solution)/shard_map/all_gather | solution.py:322
  321.2 3.8 %fusion.3 = bf16[2,32,256]{2,1,0:T(8,128)(2,1)S(1)} fusion(bf16[2,5632,256]{2,1,0:T(8,128)(2,1)} %bitcast.63, f32[1,5632,32]{1,2,0:T(8,128)S(1)} %copy-done), kind=kOutput, calls=%fused_computation.8 | convolution fusion | flops 184745984 | bytes 6520832 | tf_op jit(solution)/shard_map/cu,kus->kcs/dot_general | solution.py:324
  325.0 0.0 copy-start.4
  325.0 0.6 pad_maximum_fusion
  325.7 4.0 %all-to-all-start.1 = ((bf16[4,32,128]{2,1,0:T(8,128)(2,1)}), bf16[4,32,128]{2,1,0:T(8,128)(2,1)S(1)}, u32[]{:S(2)}, u32[]{:S(2)}) async-start(bf16[4,32,128]{2,1,0:T(8,128)(2,1)} %bitcast.15), calls=%async_computation.1 | async-start | bytes 65536 | tf_op jit(solution)/shard_map/all_to_all | solution.py:329
  329.6 0.2 select_reduce_fusion
  329.8 4.1 %all-to-all-done.1 = bf16[4,32,128]{2,1,0:T(8,128)(2,1)S(1)} async-done(((bf16[4,32,128]{2,1,0:T(8,128)(2,1)}), bf16[4,32,128]{2,1,0:T(8,128)(2,1)S(1)}, u32[]{:S(2)}, u32[]{:S(2)}) %all-to-all-start.1) | async-done | bytes 32800 | tf_op jit(solution)/shard_map/all_to_all | solution.py:329
  333.9 0.8 fusion.4
  334.7 0.9 copy.41
  335.6 0.9 copy.42
  336.4 0.9 copy.43
  (18 shorter events, 0.1 us)
Async XLA Ops:
  15.8 4.4 %copy-start = (f32[1,5632,32]{1,2,0:T(8,128)S(1)}, f32[1,5632,32]{1,2,0:T(8,128)}, u32[]{:S(2)}) copy-start(f32[1,5632,32]{1,2,0:T(8,128)} %param.13) | copy-start | bytes 2162692
  15.8 5.2 %copy-start.2 = (f32[1,32,5632]{2,1,0:T(8,128)S(1)}, f32[1,32,5632]{2,1,0:T(8,128)}, u32[]{:S(2)}) copy-start(f32[1,32,5632]{2,1,0:T(8,128)} %param.12) | copy-start | bytes 2162692
  15.8 5.2 %copy-start.6 = (f32[32]{0:T(128)S(1)}, f32[32]{0:T(128)}, u32[]{:S(2)}) copy-start(f32[32]{0:T(128)} %param.10) | copy-start | bytes 388
  15.8 154.1 %all-to-all-start = ((bf16[4,128,2048]{2,1,0:T(8,128)(2,1)}), bf16[4,128,2048]{2,1,0:T(8,128)(2,1)S(1)}, u32[]{:S(2)}, u32[]{:S(2)}) async-start(bf16[4,128,2048]{2,1,0:T(8,128)(2,1)} %bitcast.10), calls=%async_computation | async-start | bytes 4194304 | tf_op jit(solution)/shard_map/all_to_all | solution.py:312
  20.2 301.0 %all-gather.3.cloned.1.call-start = ((), (), s32[]{:S(2)}) async-start(), calls=%async_computation.2 | async-start | bytes 5857280 | tf_op jit(solution)/shard_map/all_gather | solution.py:322
  321.2 8.4 %copy-start.5 = (f32[192,2]{0,1:T(2,128)S(1)}, f32[192,2]{0,1:T(2,128)}, u32[]{:S(2)}) copy-start(f32[192,2]{0,1:T(2,128)} %param.9) | copy-start | bytes 4612
  321.2 13.5 %copy-start.1 = (bf16[176,2048]{1,0:T(8,128)(2,1)S(1)}, bf16[176,2048]{1,0:T(8,128)(2,1)}, u32[]{:S(2)}) copy-start(bf16[176,2048]{1,0:T(8,128)(2,1)} %get-tuple-element.7) | copy-start | bytes 2162692
  325.0 10.6 %copy-start.4 = (bf16[176,2048]{1,0:T(8,128)(2,1)S(1)}, bf16[176,2048]{1,0:T(8,128)(2,1)}, u32[]{:S(2)}) copy-start(bf16[176,2048]{1,0:T(8,128)(2,1)} %get-tuple-element.8) | copy-start | bytes 2162692
  325.0 11.4 %copy-start.3 = (bf16[176,2048]{1,0:T(8,128)(2,1)S(1)}, bf16[176,2048]{1,0:T(8,128)(2,1)}, u32[]{:S(2)}) copy-start(bf16[176,2048]{1,0:T(8,128)(2,1)} %get-tuple-element.9) | copy-start | bytes 2162692
  325.7 8.3 %all-to-all-start.1 = ((bf16[4,32,128]{2,1,0:T(8,128)(2,1)}), bf16[4,32,128]{2,1,0:T(8,128)(2,1)S(1)}, u32[]{:S(2)}, u32[]{:S(2)}) async-start(bf16[4,32,128]{2,1,0:T(8,128)(2,1)} %bitcast.15), calls=%async_computation.1 | async-start | bytes 65536 | tf_op jit(solution)/shard_map/all_to_all | solution.py:329
Sparse Core Ops, SparseCore 0:
  174.0 147.1 all-gather.2

commit v2 on v1

v2 whole, which is shorter than its diff:
```python
import functools

import jax
import jax.numpy as jnp
from jax import lax
from jax.experimental import pallas as pl
from jax.experimental.pallas import tpu as pltpu
from jax.sharding import Mesh
from jax.sharding import PartitionSpec as P

CAP = 128
LANES = 128
FS = ("fs_0", "fs_1")
MESH = pl.DeviceIdType.MESH
NT = (((1,), (1,)), ((), ()))


def layer_kernel(
    groups,
    chips,
    experts,
    tokens,
    routes,
    route_weight,
    gain,
    gate,
    up,
    down,
    gate_out,
    up_out,
    down_out,
    mixed_out,
    low,
    rows_buf,
    tile_buf,
    select,
    outgoing,
    arrived,
    turned,
    picked,
    split_down,
    my_down,
    hidden_all,
    partial,
    partial_in,
    column_out,
    returned,
    quad_send,
    quad_recv,
    ring_send,
    unit_recv,
    group_send,
    token_send,
    token_recv,
    core_send,
    core_recv,
    hop_send,
    hop_recv,
    back_send,
    back_recv,
):
    g = lax.axis_index("grp")
    z = lax.axis_index("fs_0")
    c = lax.axis_index("fs_1")
    t = lax.axis_index("tp")
    quads = chips // 2
    half_ring = chips // 2
    rows, hidden = gate.shape
    units = gate_out.shape[0]
    spread = groups // 2
    share = hidden // 4
    blocks = share // units
    own_count = quads // groups
    slots = experts * CAP
    q = z // 2
    odd = lax.rem(z, 2)
    me = 2 * odd + c
    half = lax.rem(g + q // spread, 2)
    active = lax.rem(q, spread) == g // 2
    pair = lax.rem(z, half_ring)
    my_block = 2 * pair + c
    my_half = my_block // (2 * blocks)
    my_source_core = lax.rem(my_block, 2 * blocks) // blocks
    parity = lax.rem(my_half + g, 2)
    own = jnp.logical_and(active, jnp.logical_and(half == my_half, c == my_source_core))
    outputs = (gate_out, up_out, down_out)
    reach = half_ring // 2

    def at(chip, core):
        return {"fs_0": chip, "fs_1": core}

    def own_quad(j):
        return spread * (2 * j + parity) + g // 2

    def sender_of(other):
        right = lax.rem(z - (2 * other + 1) + chips, chips) < half_ring
        return 2 * other + jnp.where(right, 1, 0)

    def target(i):
        chip = half * blocks + c * (blocks // 2) + i // 2
        right = lax.rem(chip - z + 2 * chips, half_ring)
        left = lax.rem(z - chip + 2 * chips, half_ring)
        chip = jnp.where(odd == 1, z + right, z - left + chips)
        return lax.rem(chip, chips), lax.rem(i, 2)

    def place(index):
        return pl.ds(pl.multiple_of(index * LANES, LANES), LANES)

    def block_rows(index):
        return pl.ds(pl.multiple_of(index * units, 16), units)

    def rows_at(index):
        return pl.ds(pl.multiple_of(index * rows, rows), rows)

    quad_mates = ((z + 1 - 2 * odd, c), (z, 1 - c), (z + 1 - 2 * odd, 1 - c))
    next_chip = lax.rem(z + 1, chips)
    last_chip = lax.rem(z + chips - 1, chips)

    barrier = pltpu.get_barrier_semaphore()

    def greet_device(where):
        pl.semaphore_signal(barrier, inc=1, device_id=where, device_id_type=MESH)

    def greet(j, _):
        other = own_quad(j)
        chip = sender_of(other)

        @pl.when(jnp.logical_not(jnp.logical_and(own, other == q)))
        def _():
            greet_device(at(chip, my_source_core))

        return 0

    lax.fori_loop(0, own_count, greet, 0)
    for chip, core in quad_mates:
        greet_device(at(chip, core))
    for step in range(1, groups):
        greet_device({"grp": lax.rem(g + step, groups)})
    for step in range(1, experts):
        greet_device({"tp": lax.rem(t + step, experts)})
    greet_device(at(next_chip, c))
    greet_device(at(last_chip, c))

    eye = lax.broadcasted_iota(jnp.int32, (rows, rows), 0) == lax.broadcasted_iota(
        jnp.int32, (rows, rows), 1
    )
    gain_column = jnp.sum(jnp.where(eye, gain[...], 0.0), axis=1, keepdims=True)
    low[0, :, :] = (gate[...] * gain_column).astype(jnp.bfloat16)
    low[1, :, :] = (up[...] * gain_column).astype(jnp.bfloat16)
    low[2, :, :] = down[...].astype(jnp.bfloat16)

    token_count, width = tokens.shape
    first = routes[0:1, :]
    second = routes[1:2, :]
    expert_row = lax.broadcasted_iota(jnp.int32, (8, token_count), 0)
    named = jnp.logical_or(first == expert_row, second == expert_row)
    before = (
        lax.broadcasted_iota(jnp.int32, (token_count, token_count), 0)
        < lax.broadcasted_iota(jnp.int32, (token_count, token_count), 1)
    )
    rank = jnp.dot(
        jnp.where(named, 1.0, 0.0).astype(jnp.bfloat16),
        jnp.where(before, 1.0, 0.0).astype(jnp.bfloat16),
        preferred_element_type=jnp.float32,
    )
    slot = lax.broadcasted_iota(jnp.int32, (CAP, token_count), 0).astype(jnp.float32)
    tok_float = tokens[...].astype(jnp.float32)
    normed = (
        tok_float * lax.rsqrt(jnp.mean(tok_float * tok_float, axis=-1, keepdims=True) + 1e-06)
    ).astype(jnp.bfloat16)
    for e in range(experts):
        chosen = jnp.logical_or(first == e, second == e)
        hot = jnp.logical_and(slot == rank[e : e + 1, :], chosen)
        select[e, :, :] = jnp.where(hot, 1.0, 0.0).astype(jnp.bfloat16)
        outgoing[e, :, :] = jnp.dot(
            select[e, :, :], normed, preferred_element_type=jnp.float32
        ).astype(jnp.bfloat16)

    expected = jnp.where(active, blocks - jnp.where(own, 1, 0), 0)
    pl.semaphore_wait(barrier, expected + groups - 1 + 3 + experts - 1 + 2)

    def lanes_for(core):
        return pl.ds(pl.multiple_of((2 * half + core) * share, LANES), share)

    def mate_copy(m, k):
        chip, core = quad_mates[k]
        return pltpu.make_async_remote_copy(
            src_ref=low.at[m, :, lanes_for(core)],
            dst_ref=rows_buf.at[m, rows_at(me), :],
            send_sem=quad_send.at[m, k],
            recv_sem=quad_recv.at[m, me],
            device_id=at(chip, core),
            device_id_type=MESH,
        )

    def ring_copy(m, i):
        chip, core = target(i)
        return pltpu.make_async_remote_copy(
            src_ref=tile_buf.at[m, block_rows(i), :],
            dst_ref=outputs[m].at[:, place(q)],
            send_sem=ring_send.at[m, i],
            recv_sem=unit_recv.at[m, q],
            device_id=at(chip, core),
            device_id_type=MESH,
        )

    def group_copy(m, j, step):
        other = own_quad(j)
        return pltpu.make_async_remote_copy(
            src_ref=outputs[m].at[:, place(other)],
            dst_ref=outputs[m].at[:, place(other)],
            send_sem=group_send.at[m, j, step - 1],
            recv_sem=unit_recv.at[m, other],
            device_id={"grp": lax.rem(g + step, groups)},
            device_id_type=MESH,
        )

    def unit_arrival(m, index):
        return pltpu.make_async_remote_copy(
            src_ref=outputs[m].at[:, place(index)],
            dst_ref=outputs[m].at[:, place(index)],
            send_sem=group_send.at[m, 0, 0],
            recv_sem=unit_recv.at[m, index],
            device_id={"grp": lax.rem(g + 1, groups)},
            device_id_type=MESH,
        )

    def is_mine(i):
        chip, core = target(i)
        return jnp.logical_and(chip == z, core == c)

    def token_copy(step):
        other = lax.rem(t + step, experts)
        return pltpu.make_async_remote_copy(
            src_ref=outgoing.at[other],
            dst_ref=arrived.at[t],
            send_sem=token_send.at[step - 1],
            recv_sem=token_recv.at[t],
            device_id={"tp": other},
            device_id_type=MESH,
        )

    def token_arrival(step):
        other = lax.rem(t + step, experts)
        return pltpu.make_async_remote_copy(
            src_ref=outgoing.at[other],
            dst_ref=arrived.at[other],
            send_sem=token_send.at[step - 1],
            recv_sem=token_recv.at[other],
            device_id={"tp": other},
            device_id_type=MESH,
        )

    @pl.when(active)
    def _():
        for m in range(3):
            for k in range(3):
                mate_copy(m, k).start()
        for step in range(1, experts):
            token_copy(step).start()
        for m in range(3):
            rows_buf[m, rows_at(me), :] = low[m, :, lanes_for(c)]
            for k in range(3):
                chip_back, core_back = quad_mates[k]
                source = 2 * lax.rem(chip_back, 2) + core_back
                pltpu.make_async_remote_copy(
                    src_ref=low.at[m, :, lanes_for(c)],
                    dst_ref=rows_buf.at[m, rows_at(source), :],
                    send_sem=quad_send.at[m, k],
                    recv_sem=quad_recv.at[m, source],
                    device_id=at(chip_back, core_back),
                    device_id_type=MESH,
                ).wait_recv()
            tile_buf[m, :, :] = rows_buf[m, :, :].T

            def send(i, _):
                mine = is_mine(i)

                @pl.when(mine)
                def _():
                    outputs[m][:, place(q)] = tile_buf[m, block_rows(i), :]

                @pl.when(jnp.logical_not(mine))
                def _():
                    ring_copy(m, i).start()

                return 0

            lax.fori_loop(0, blocks, send, 0)

    @pl.when(jnp.logical_not(active))
    def _():
        for step in range(1, experts):
            token_copy(step).start()

    arrived[t] = outgoing[t]

    chunk = 4 * LANES

    def turn(k, _):
        lanes = pl.ds(pl.multiple_of(k * chunk, chunk), chunk)
        tall = jnp.concatenate(
            [down[:, lanes], jnp.zeros((LANES - rows, chunk), jnp.float32)], axis=0
        )
        turned[lanes, :] = tall.T.astype(jnp.bfloat16)
        return 0

    lax.fori_loop(0, hidden // chunk, turn, 0)

    def pick(k, _):
        for p in range(2):
            picked[p, block_rows(k), :] = turned[block_rows(2 * k + p), :]
        return 0

    lax.fori_loop(0, half_ring, pick, 0)
    piece = 2 * LANES

    def lay(k, _):
        span = pl.ds(pl.multiple_of(k * piece, piece), piece)
        for p in range(2):
            split_down[p, :, span] = picked[p, span, :].T[:rows, :]
        return 0

    lax.fori_loop(0, hidden // 2 // piece, lay, 0)
    my_down[rows_at(c), :] = split_down[c]
    columns_copy = pltpu.make_async_remote_copy(
        src_ref=split_down.at[1 - c],
        dst_ref=my_down.at[rows_at(c), :],
        send_sem=core_send.at[0],
        recv_sem=core_recv.at[0],
        device_id=at(z, 1 - c),
        device_id_type=MESH,
    )
    columns_copy.start()

    def forward(m, j):
        other = own_quad(j)

        @pl.when(jnp.logical_not(jnp.logical_and(own, other == q)))
        def _():
            unit_arrival(m, other).wait_recv()

        for step in range(1, groups):
            group_copy(m, j, step).start()

    def arrive(m):
        def body(index, _):
            here = jnp.logical_and(
                lax.rem(index, spread) == g // 2, lax.rem(index // spread, 2) == parity
            )

            @pl.when(jnp.logical_not(here))
            def _():
                unit_arrival(m, index).wait_recv()

            return 0

        lax.fori_loop(0, quads, body, 0)

    for m in range(2):

        def body(j, _):
            forward(m, j)
            return 0

        lax.fori_loop(0, own_count, body, 0)
    for m in range(2):
        arrive(m)
    for step in range(1, experts):
        token_arrival(step).wait_recv()

    wide = slots // 2

    def hide(k, _):
        own_tokens = arrived[pl.ds(k * (experts // 2), experts // 2)].reshape(wide, width)
        gated = lax.dot_general(gate_out[...], own_tokens, NT, preferred_element_type=jnp.float32)
        lifted = lax.dot_general(up_out[...], own_tokens, NT, preferred_element_type=jnp.float32)
        hidden_all[k, block_rows(pair), :] = (
            gated * (1.0 / (1.0 + jnp.exp(-gated))) * lifted
        ).astype(jnp.bfloat16)
        return 0

    lax.fori_loop(0, 2, hide, 0)

    def hop_copy(way, k, step):
        chip = lax.rem(z + chips - step if way == 0 else z + step, half_ring)
        return pltpu.make_async_remote_copy(
            src_ref=hidden_all.at[k, block_rows(chip), :],
            dst_ref=hidden_all.at[k, block_rows(chip), :],
            send_sem=hop_send.at[way, k, step],
            recv_sem=hop_recv.at[way, k, step],
            device_id=at(next_chip if way == 0 else last_chip, c),
            device_id_type=MESH,
        )

    def hop_arrival(way, k, step):
        chip = lax.rem(z + chips - step - 1 if way == 0 else z + step + 1, half_ring)
        return pltpu.make_async_remote_copy(
            src_ref=hidden_all.at[k, block_rows(chip), :],
            dst_ref=hidden_all.at[k, block_rows(chip), :],
            send_sem=hop_send.at[way, k, step],
            recv_sem=hop_recv.at[way, k, step],
            device_id=at(last_chip if way == 0 else next_chip, c),
            device_id_type=MESH,
        )

    for k in range(2):
        for way in range(2):
            hop_copy(way, k, 0).start()

    def hop(step, _):
        @pl.when(step < own_count)
        def _():
            forward(2, step)

        for k in range(2):
            for way in range(2):
                hop_arrival(way, k, step).wait_recv()

                @pl.when(jnp.logical_or(step < reach - 2, k == way))
                def _():
                    hop_copy(way, k, step + 1).start()

        return 0

    lax.fori_loop(0, reach - 1, hop, 0)
    for j in range(reach - 1, own_count):
        forward(2, j)
    for way in range(2):
        hop_arrival(way, way, reach - 1).wait_recv()
    columns_copy.wait()

    for k in range(2):
        partial[k, :, :] = jnp.dot(
            my_down[...], hidden_all[k, :, :], preferred_element_type=jnp.float32
        )

    partial_copy = pltpu.make_async_remote_copy(
        src_ref=partial.at[:, rows_at(1 - c), :],
        dst_ref=partial_in,
        send_sem=core_send.at[1],
        recv_sem=core_recv.at[1],
        device_id=at(z, 1 - c),
        device_id_type=MESH,
    )
    partial_copy.start()
    partial_copy.wait_recv()
    for e in range(experts):
        k, lane = e // (experts // 2), (e % (experts // 2)) * CAP
        lanes = pl.ds(lane, CAP)
        column_out[e, :, :] = (
            partial[k, rows_at(c), lanes] + partial_in[k, :, lanes]
        ).astype(jnp.bfloat16)

    def back_copy(step):
        other = lax.rem(t + step, experts)
        return pltpu.make_async_remote_copy(
            src_ref=column_out.at[other],
            dst_ref=returned.at[t],
            send_sem=back_send.at[step - 1],
            recv_sem=back_recv.at[t],
            device_id={"tp": other},
            device_id_type=MESH,
        )

    def back_arrival(step):
        other = lax.rem(t + step, experts)
        return pltpu.make_async_remote_copy(
            src_ref=column_out.at[other],
            dst_ref=returned.at[other],
            send_sem=back_send.at[step - 1],
            recv_sem=back_recv.at[other],
            device_id={"tp": other},
            device_id_type=MESH,
        )

    for step in range(1, experts):
        back_copy(step).start()
    returned[t] = column_out[t]
    for step in range(1, experts):
        back_arrival(step).wait_recv()
    total = jnp.zeros((rows, token_count), jnp.float32)
    for e in range(experts):
        weight = jnp.where(first == e, route_weight[0:1, :], 0.0) + jnp.where(
            second == e, route_weight[1:2, :], 0.0
        )
        total = total + weight * jnp.dot(
            returned[e, :, :], select[e, :, :], preferred_element_type=jnp.float32
        )
    mixed_out[...] = total.astype(jnp.bfloat16)

    arrive(2)
    for m in range(3):

        @pl.when(active)
        def _():
            for k in range(3):
                mate_copy(m, k).wait_send()

            def sent(i, _):
                @pl.when(jnp.logical_not(is_mine(i)))
                def _():
                    ring_copy(m, i).wait_send()

                return 0

            lax.fori_loop(0, blocks, sent, 0)

        def passed(j, _):
            for step in range(1, groups):
                group_copy(m, j, step).wait_send()
            return 0

        lax.fori_loop(0, own_count, passed, 0)

    def hopped(step, _):
        for k in range(2):
            for way in range(2):

                @pl.when(jnp.logical_or(step < reach - 1, k == way))
                def _():
                    hop_copy(way, k, step).wait_send()

        return 0

    lax.fori_loop(0, reach, hopped, 0)
    partial_copy.wait_send()
    for step in range(1, experts):
        token_copy(step).wait_send()
        back_copy(step).wait_send()


def layer(groups, chips, experts, *operands):
    tokens, _, _, _, gate, _, _ = operands
    rows, hidden = gate.shape
    units = hidden // chips
    width = rows * 2 * chips
    quads = chips // 2
    share = hidden // 4
    reach = chips // 4
    wide = experts * CAP // 2
    served = jax.ShapeDtypeStruct((units, width), jnp.bfloat16)
    dma = pltpu.SemaphoreType.DMA
    return pl.pallas_call(
        functools.partial(layer_kernel, groups, chips, experts),
        out_shape=(
            served,
            served,
            served,
            jax.ShapeDtypeStruct((rows, tokens.shape[0]), jnp.bfloat16),
        ),
        in_specs=[pl.BlockSpec(memory_space=pltpu.VMEM)] * 7,
        out_specs=[pl.BlockSpec(memory_space=pltpu.VMEM)] * 4,
        scratch_shapes=[
            pltpu.VMEM((3, rows, hidden), jnp.bfloat16),
            pltpu.VMEM((3, 4 * rows, share), jnp.bfloat16),
            pltpu.VMEM((3, share, 4 * rows), jnp.bfloat16),
            pltpu.VMEM((experts, CAP, tokens.shape[0]), jnp.bfloat16),
            pltpu.VMEM((experts, CAP, width), jnp.bfloat16),
            pltpu.VMEM((experts, CAP, width), jnp.bfloat16),
            pltpu.VMEM((hidden, LANES), jnp.bfloat16),
            pltpu.VMEM((2, hidden // 2, LANES), jnp.bfloat16),
            pltpu.VMEM((2, rows, hidden // 2), jnp.bfloat16),
            pltpu.VMEM((2 * rows, hidden // 2), jnp.bfloat16),
            pltpu.VMEM((2, hidden // 2, wide), jnp.bfloat16),
            pltpu.VMEM((2, 2 * rows, wide), jnp.float32),
            pltpu.VMEM((2, rows, wide), jnp.float32),
            pltpu.VMEM((experts, rows, CAP), jnp.bfloat16),
            pltpu.VMEM((experts, rows, CAP), jnp.bfloat16),
            dma((3, 3)),
            dma((3, 4)),
            dma((3, share // units)),
            dma((3, quads)),
            dma((3, quads // groups, groups - 1)),
            dma((experts - 1,)),
            dma((experts,)),
            dma((2,)),
            dma((2,)),
            dma((2, 2, reach)),
            dma((2, 2, reach)),
            dma((experts - 1,)),
            dma((experts,)),
        ],
        compiler_params=pltpu.CompilerParams(
            collective_id=0, has_side_effects=True, vmem_limit_bytes=48 * 1024 * 1024
        ),
        name="layer",
    )(*operands)


def shards(tokens, routes, route_weight, norm_gain, gate_train, up_train, down_train):
    gate_new, up_new, down_new, mixed = layer(
        lax.axis_size("grp"),
        lax.axis_size("fs_0"),
        lax.axis_size("tp"),
        tokens,
        routes.T,
        route_weight.T,
        norm_gain[None, :],
        gate_train[0],
        up_train[0],
        down_train[0].T,
    )
    return (gate_new.T[None], up_new.T[None], down_new[None], mixed.T)


def solution(mesh):
    cores = 2
    split = Mesh(
        mesh.devices.reshape(
            mesh.shape["grp"], mesh.shape["fs"] // cores, cores, mesh.shape["tp"]
        ),
        ("grp", "fs_0", "fs_1", "tp"),
    )
    placed = (
        P(("grp", "tp"), None),
        P(("grp", "tp"), None),
        P(("grp", "tp"), None),
        P(FS),
        P("tp", FS, None),
        P("tp", FS, None),
        P("tp", None, FS),
    )
    return jax.shard_map(
        shards,
        mesh=split,
        in_specs=placed,
        out_specs=(
            P(("grp", "tp"), None, FS),
            P(("grp", "tp"), None, FS),
            P(("grp", "tp"), FS, None),
            P(("grp", "tp"), FS),
        ),
        check_vma=False,
    )
```

time: 346 us -> 209 us (0.60)
  waiting for transfers between devices: 152 us -> 0 us
  Pallas kernels: 147 us -> 199 us
  between operations: 14.1 us -> 0.67 us
  matrix products: 11.7 us -> 0 us
  starting transfers between devices: 8.43 us -> 0 us
  other arithmetic: 7.4 us -> 0 us
  local copies, waits for them, and re-layouts: 4.13 us -> 8.32 us
    all_gather x1 -> x0, waiting for transfers between devices: 147 us -> none  [shards(): every = lax.all_gather(hidden, FS)]
    pallas_call x1, Pallas kernels: 147 us -> 199 us  [layer(): pl.pallas_call(functools.partial(layer_kernel, groups, chips, experts), o...]
    dot_general x5 -> x0, matrix products: 11.7 us -> none  [the longest x1 3.78 us: shards(): jnp.einsum('cu,kus->kcs', down_low, every, preferred_element_type=jnp.flo...]
    all_to_all x2 -> x0, starting transfers between devices: 8.42 us -> none  [the longest x1 4.43 us: shards(): lax.all_to_all(outgoing, 'tp', split_axis=0, concat_axis=0, tiled=True)]
    unnamed x18, local copies, waits for them, and re-layouts: 3.4 us -> 8.32 us
    all_to_all x2 -> x0, waiting for transfers between devices: 4.12 us -> none  [the longest x1 4.12 us: shards(): lax.all_to_all(back.reshape(EXPERTS, columns, CAP), 'tp', split_axis=0, c...]
  transfers between devices with their start and end apart: 3 -> 0, of which waited for: 2 -> 0; matrix products, arithmetic and copies ran while one was open for 1% -> 0% of each run, Pallas kernels for 43% -> 0%
where the time goes in v2:
time: 209 us; the launch traced here: 208 us
  Pallas kernels  199 us (95%)
  local copies, waits for them, and re-layouts  8.32 us (4%)
    pallas_call x1, Pallas kernels, layer(): pl.pallas_call(functools.partial(layer_kernel, groups, chips, experts), o...  199 us
    unnamed x18, local copies, waits for them, and re-layouts  8.32 us

profile of v2, /device:TPU:41, one launch (start us, length us, event | category | flops | bytes accessed | tf_op | source)
XLA Modules:
  0.0 208.2 jit_solution(4239305113136742317)
XLA Ops:
  0.6 0.0 copy-start.5
  0.6 0.0 copy-start.4
  0.7 0.0 copy-start.6
  0.7 0.7 copy-done.5
  1.3 0.0 copy-done.4
  1.3 0.0 copy-done.6
  1.3 0.0 copy-start
  1.3 1.1 copy-done
  2.5 0.0 copy-start.1
  2.5 1.1 copy-done.1
  3.6 0.0 copy-start.2
  3.6 1.1 copy-done.2
  4.7 0.0 copy-start.3
  4.7 1.1 copy-done.3
  5.8 199.2 %layer.1 = (bf16[176,2048]{1,0:T(8,128)(2,1)S(1)}, bf16[176,2048]{1,0:T(8,128)(2,1)S(1)}, bf16[176,2048]{1,0:T(8,128)(2,1)S(1)}, bf16[32,192]{1,0:T(8,128)(2,1)S(1)}) custom-call(bf16[192,2048]{1,0:T(8,128)(2,1)S(1)} %copy-done, s32[2,192]{1,0:T(2,128)S(1)} %bitcast.23, f32[2,192]{1,0:T(2,128)S(1)} %bitcast.24, f32[1,32]{1,0:T(1,128)S(1)} %bitcast.25, ...), custom_call_target="tpu_custom_call" | custom-call | tf_op jit(solution)/shard_map/layer/pallas_call | solution.py:544
  205.0 0.9 copy.15
  205.9 0.9 copy.16
  206.7 0.9 copy.17
  207.6 0.6 copy.18
Async XLA Ops:
  0.6 0.7 copy-start.5
  0.6 0.7 copy-start.4
  0.7 0.7 copy-start.6
  1.3 1.1 copy-start
  2.5 1.1 copy-start.1
  3.6 1.1 copy-start.2
  4.7 1.1 copy-start.3

commit v3 on v2

--- a/solution.py
+++ b/solution.py
@@ -12,6 +12,7 @@
 LANES = 128
 FS = ("fs_0", "fs_1")
 MESH = pl.DeviceIdType.MESH
+SUB = 2
 NT = (((1,), (1,)), ((), ()))
 
 
@@ -19,17 +20,19 @@
     groups,
     chips,
     experts,
-    tokens,
     routes,
     route_weight,
     gain,
-    gate,
-    up,
-    down,
+    tokens_far,
+    gate_far,
+    up_far,
+    down_far,
     gate_out,
     up_out,
     down_out,
     mixed_out,
+    tokens,
+    full,
     low,
     rows_buf,
     tile_buf,
@@ -58,6 +61,7 @@
     hop_recv,
     back_send,
     back_recv,
+    read_sem,
 ):
     g = lax.axis_index("grp")
     z = lax.axis_index("fs_0")
@@ -65,7 +69,7 @@
     t = lax.axis_index("tp")
     quads = chips // 2
     half_ring = chips // 2
-    rows, hidden = gate.shape
+    rows, hidden = gate_far.shape
     units = gate_out.shape[0]
     spread = groups // 2
     share = hidden // 4
@@ -92,6 +96,15 @@
     def own_quad(j):
         return spread * (2 * j + parity) + g // 2
 
+    stride = blocks // own_count
+
+    def turn_of(other):
+        return lax.rem(other // spread // 2, own_count) * stride
+
+    def expected_quad(n):
+        place_in_list = lax.rem(my_block, blocks) // stride
+        return own_quad(lax.rem(place_in_list - n + own_count, own_count))
+
     def sender_of(other):
         right = lax.rem(z - (2 * other + 1) + chips, chips) < half_ring
         return 2 * other + jnp.where(right, 1, 0)
@@ -115,6 +128,14 @@
     quad_mates = ((z + 1 - 2 * odd, c), (z, 1 - c), (z + 1 - 2 * odd, 1 - c))
     next_chip = lax.rem(z + 1, chips)
     last_chip = lax.rem(z + chips - 1, chips)
+
+    reads = [
+        pltpu.make_async_copy(far, full.at[m], read_sem.at[m])
+        for m, far in enumerate((gate_far, up_far, down_far))
+    ]
+    reads.append(pltpu.make_async_copy(tokens_far, tokens, read_sem.at[3]))
+    for read in reads:
+        read.start()
 
     barrier = pltpu.get_barrier_semaphore()
 
@@ -145,9 +166,92 @@
         jnp.int32, (rows, rows), 1
     )
     gain_column = jnp.sum(jnp.where(eye, gain[...], 0.0), axis=1, keepdims=True)
-    low[0, :, :] = (gate[...] * gain_column).astype(jnp.bfloat16)
-    low[1, :, :] = (up[...] * gain_column).astype(jnp.bfloat16)
-    low[2, :, :] = down[...].astype(jnp.bfloat16)
+    for m in range(2):
+        reads[m].wait()
+        low[m, :, :] = (full[m] * gain_column).astype(jnp.bfloat16)
+    reads[2].wait()
+    low[2, :, :] = full[2].astype(jnp.bfloat16)
+
+    expected = jnp.where(active, blocks - jnp.where(own, 1, 0), 0)
+    pl.semaphore_wait(barrier, expected + groups - 1 + 3 + experts - 1 + 2)
+
+    def lanes_for(core):
+        return pl.ds(pl.multiple_of((2 * half + core) * share, LANES), share)
+
+    def mate_copy(m, k):
+        chip, core = quad_mates[k]
+        return pltpu.make_async_remote_copy(
+            src_ref=low.at[m, :, lanes_for(core)],
+            dst_ref=rows_buf.at[m, rows_at(me), :],
+            send_sem=quad_send.at[m, k],
+            recv_sem=quad_recv.at[m, me],
+            device_id=at(chip, core),
+            device_id_type=MESH,
+        )
+
+    def ring_copy(m, i):
+        chip, core = target(i)
+        return pltpu.make_async_remote_copy(
+            src_ref=tile_buf.at[m, block_rows(i), :],
+            dst_ref=outputs[m].at[:, place(q)],
+            send_sem=ring_send.at[m, i],
+            recv_sem=unit_recv.at[m, q],
+            device_id=at(chip, core),
+            device_id_type=MESH,
+        )
+
+    def group_copy(m, j, step):
+        other = expected_quad(j)
+        return pltpu.make_async_remote_copy(
+            src_ref=outputs[m].at[:, place(other)],
+            dst_ref=outputs[m].at[:, place(other)],
+            send_sem=group_send.at[m, j, step - 1],
+            recv_sem=unit_recv.at[m, other],
+            device_id={"grp": lax.rem(g + step, groups)},
+            device_id_type=MESH,
+        )
+
+    def unit_arrival(m, index):
+        return pltpu.make_async_remote_copy(
+            src_ref=outputs[m].at[:, place(index)],
+            dst_ref=outputs[m].at[:, place(index)],
+            send_sem=group_send.at[m, 0, 0],
+            recv_sem=unit_recv.at[m, index],
+            device_id={"grp": lax.rem(g + 1, groups)},
+            device_id_type=MESH,
+        )
+
+    def is_mine(i):
+        chip, core = target(i)
+        return jnp.logical_and(chip == z, core == c)
+
+    def token_copy(step):
+        other = lax.rem(t + step, experts)
+        return pltpu.make_async_remote_copy(
+            src_ref=outgoing.at[other],
+            dst_ref=arrived.at[t],
+            send_sem=token_send.at[step - 1],
+            recv_sem=token_recv.at[t],
+            device_id={"tp": other},
+            device_id_type=MESH,
+        )
+
+    def token_arrival(step):
+        other = lax.rem(t + step, experts)
+        return pltpu.make_async_remote_copy(
+            src_ref=outgoing.at[other],
+            dst_ref=arrived.at[other],
+            send_sem=token_send.at[step - 1],
+            recv_sem=token_recv.at[other],
+            device_id={"tp": other},
+            device_id_type=MESH,
+        )
+
+    @pl.when(active)
+    def _():
+        for m in range(3):
+            for k in range(3):
+                mate_copy(m, k).start()
 
     token_count, width = tokens.shape
     first = routes[0:1, :]
@@ -164,6 +268,7 @@
         preferred_element_type=jnp.float32,
     )
     slot = lax.broadcasted_iota(jnp.int32, (CAP, token_count), 0).astype(jnp.float32)
+    reads[3].wait()
     tok_float = tokens[...].astype(jnp.float32)
     normed = (
         tok_float * lax.rsqrt(jnp.mean(tok_float * tok_float, axis=-1, keepdims=True) + 1e-06)
@@ -176,88 +281,12 @@
             select[e, :, :], normed, preferred_element_type=jnp.float32
         ).astype(jnp.bfloat16)
 
-    expected = jnp.where(active, blocks - jnp.where(own, 1, 0), 0)
-    pl.semaphore_wait(barrier, expected + groups - 1 + 3 + experts - 1 + 2)
-
-    def lanes_for(core):
-        return pl.ds(pl.multiple_of((2 * half + core) * share, LANES), share)
-
-    def mate_copy(m, k):
-        chip, core = quad_mates[k]
-        return pltpu.make_async_remote_copy(
-            src_ref=low.at[m, :, lanes_for(core)],
-            dst_ref=rows_buf.at[m, rows_at(me), :],
-            send_sem=quad_send.at[m, k],
-            recv_sem=quad_recv.at[m, me],
-            device_id=at(chip, core),
-            device_id_type=MESH,
-        )
-
-    def ring_copy(m, i):
-        chip, core = target(i)
-        return pltpu.make_async_remote_copy(
-            src_ref=tile_buf.at[m, block_rows(i), :],
-            dst_ref=outputs[m].at[:, place(q)],
-            send_sem=ring_send.at[m, i],
-            recv_sem=unit_recv.at[m, q],
-            device_id=at(chip, core),
-            device_id_type=MESH,
-        )
-
-    def group_copy(m, j, step):
-        other = own_quad(j)
-        return pltpu.make_async_remote_copy(
-            src_ref=outputs[m].at[:, place(other)],
-            dst_ref=outputs[m].at[:, place(other)],
-            send_sem=group_send.at[m, j, step - 1],
-            recv_sem=unit_recv.at[m, other],
-            device_id={"grp": lax.rem(g + step, groups)},
-            device_id_type=MESH,
-        )
-
-    def unit_arrival(m, index):
-        return pltpu.make_async_remote_copy(
-            src_ref=outputs[m].at[:, place(index)],
-            dst_ref=outputs[m].at[:, place(index)],
-            send_sem=group_send.at[m, 0, 0],
-            recv_sem=unit_recv.at[m, index],
-            device_id={"grp": lax.rem(g + 1, groups)},
-            device_id_type=MESH,
-        )
-
-    def is_mine(i):
-        chip, core = target(i)
-        return jnp.logical_and(chip == z, core == c)
-
-    def token_copy(step):
-        other = lax.rem(t + step, experts)
-        return pltpu.make_async_remote_copy(
-            src_ref=outgoing.at[other],
-            dst_ref=arrived.at[t],
-            send_sem=token_send.at[step - 1],
-            recv_sem=token_recv.at[t],
-            device_id={"tp": other},
-            device_id_type=MESH,
-        )
-
-    def token_arrival(step):
-        other = lax.rem(t + step, experts)
-        return pltpu.make_async_remote_copy(
-            src_ref=outgoing.at[other],
-            dst_ref=arrived.at[other],
-            send_sem=token_send.at[step - 1],
-            recv_sem=token_recv.at[other],
-            device_id={"tp": other},
-            device_id_type=MESH,
-        )
+    for step in range(1, experts):
+        token_copy(step).start()
+    arrived[t] = outgoing[t]
 
     @pl.when(active)
     def _():
-        for m in range(3):
-            for k in range(3):
-                mate_copy(m, k).start()
-        for step in range(1, experts):
-            token_copy(step).start()
         for m in range(3):
             rows_buf[m, rows_at(me), :] = low[m, :, lanes_for(c)]
             for k in range(3):
@@ -273,7 +302,8 @@
                 ).wait_recv()
             tile_buf[m, :, :] = rows_buf[m, :, :].T
 
-            def send(i, _):
+            def send(n, _):
+                i = lax.rem(n + turn_of(q), blocks)
                 mine = is_mine(i)
 
                 @pl.when(mine)
@@ -288,19 +318,13 @@
 
             lax.fori_loop(0, blocks, send, 0)
 
-    @pl.when(jnp.logical_not(active))
-    def _():
-        for step in range(1, experts):
-            token_copy(step).start()
-
-    arrived[t] = outgoing[t]
 
     chunk = 4 * LANES
 
     def turn(k, _):
         lanes = pl.ds(pl.multiple_of(k * chunk, chunk), chunk)
         tall = jnp.concatenate(
-            [down[:, lanes], jnp.zeros((LANES - rows, chunk), jnp.float32)], axis=0
+            [full[2, :, lanes], jnp.zeros((LANES - rows, chunk), jnp.float32)], axis=0
         )
         turned[lanes, :] = tall.T.astype(jnp.bfloat16)
         return 0
@@ -334,7 +358,7 @@
     columns_copy.start()
 
     def forward(m, j):
-        other = own_quad(j)
+        other = expected_quad(j)
 
         @pl.when(jnp.logical_not(jnp.logical_and(own, other == q)))
         def _():
@@ -382,31 +406,34 @@
 
     lax.fori_loop(0, 2, hide, 0)
 
-    def hop_copy(way, k, step):
+    part = wide // SUB
+
+    def hop_copy(way, k, step, j):
         chip = lax.rem(z + chips - step if way == 0 else z + step, half_ring)
         return pltpu.make_async_remote_copy(
-            src_ref=hidden_all.at[k, block_rows(chip), :],
-            dst_ref=hidden_all.at[k, block_rows(chip), :],
-            send_sem=hop_send.at[way, k, step],
-            recv_sem=hop_recv.at[way, k, step],
+            src_ref=hidden_all.at[k, block_rows(chip), pl.ds(j * part, part)],
+            dst_ref=hidden_all.at[k, block_rows(chip), pl.ds(j * part, part)],
+            send_sem=hop_send.at[way, k, step, j],
+            recv_sem=hop_recv.at[way, k, step, j],
             device_id=at(next_chip if way == 0 else last_chip, c),
             device_id_type=MESH,
         )
 
-    def hop_arrival(way, k, step):
+    def hop_arrival(way, k, step, j):
         chip = lax.rem(z + chips - step - 1 if way == 0 else z + step + 1, half_ring)
         return pltpu.make_async_remote_copy(
-            src_ref=hidden_all.at[k, block_rows(chip), :],
-            dst_ref=hidden_all.at[k, block_rows(chip), :],
-            send_sem=hop_send.at[way, k, step],
-            recv_sem=hop_recv.at[way, k, step],
+            src_ref=hidden_all.at[k, block_rows(chip), pl.ds(j * part, part)],
+            dst_ref=hidden_all.at[k, block_rows(chip), pl.ds(j * part, part)],
+            send_sem=hop_send.at[way, k, step, j],
+            recv_sem=hop_recv.at[way, k, step, j],
             device_id=at(last_chip if way == 0 else next_chip, c),
             device_id_type=MESH,
         )
 
     for k in range(2):
-        for way in range(2):
-            hop_copy(way, k, 0).start()
+        for j in range(SUB):
+            for way in range(2):
+                hop_copy(way, k, 0, j).start()
 
     def hop(step, _):
         @pl.when(step < own_count)
@@ -414,12 +441,13 @@
             forward(2, step)
 
         for k in range(2):
-            for way in range(2):
-                hop_arrival(way, k, step).wait_recv()
-
-                @pl.when(jnp.logical_or(step < reach - 2, k == way))
-                def _():
-                    hop_copy(way, k, step + 1).start()
+            for j in range(SUB):
+                for way in range(2):
+                    hop_arrival(way, k, step, j).wait_recv()
+
+                    @pl.when(jnp.logical_or(step < reach - 2, k == way))
+                    def _():
+                        hop_copy(way, k, step + 1, j).start()
 
         return 0
 
@@ -427,7 +455,8 @@
     for j in range(reach - 1, own_count):
         forward(2, j)
     for way in range(2):
-        hop_arrival(way, way, reach - 1).wait_recv()
+        for j in range(SUB):
+            hop_arrival(way, way, reach - 1, j).wait_recv()
     columns_copy.wait()
 
     for k in range(2):
@@ -519,7 +548,8 @@
 
                 @pl.when(jnp.logical_or(step < reach - 1, k == way))
                 def _():
-                    hop_copy(way, k, step).wait_send()
+                    for j in range(SUB):
+                        hop_copy(way, k, step, j).wait_send()
 
         return 0
 
@@ -531,7 +561,7 @@
 
 
 def layer(groups, chips, experts, *operands):
-    tokens, _, _, _, gate, _, _ = operands
+    tokens, gate = operands[3], operands[4]
     rows, hidden = gate.shape
     units = hidden // chips
     width = rows * 2 * chips
@@ -549,9 +579,12 @@
             served,
             jax.ShapeDtypeStruct((rows, tokens.shape[0]), jnp.bfloat16),
         ),
-        in_specs=[pl.BlockSpec(memory_space=pltpu.VMEM)] * 7,
+        in_specs=[pl.BlockSpec(memory_space=pltpu.VMEM)] * 3
+        + [pl.BlockSpec(memory_space=pltpu.HBM)] * 4,
         out_specs=[pl.BlockSpec(memory_space=pltpu.VMEM)] * 4,
         scratch_shapes=[
+            pltpu.VMEM(tokens.shape, jnp.bfloat16),
+            pltpu.VMEM((3, rows, hidden), jnp.float32),
             pltpu.VMEM((3, rows, hidden), jnp.bfloat16),
             pltpu.VMEM((3, 4 * rows, share), jnp.bfloat16),
             pltpu.VMEM((3, share, 4 * rows), jnp.bfloat16),
@@ -576,31 +609,57 @@
             dma((experts,)),
             dma((2,)),
             dma((2,)),
-            dma((2, 2, reach)),
-            dma((2, 2, reach)),
+            dma((2, 2, reach, SUB)),
+            dma((2, 2, reach, SUB)),
             dma((experts - 1,)),
             dma((experts,)),
+            dma((4,)),
         ],
         compiler_params=pltpu.CompilerParams(
-            collective_id=0, has_side_effects=True, vmem_limit_bytes=48 * 1024 * 1024
+            collective_id=0, has_side_effects=True, vmem_limit_bytes=52736 * 1024
         ),
         name="layer",
     )(*operands)
 
 
+def store_kernel(*refs):
+    count = len(refs) // 2
+    sem = refs[-1]
+    copies = [
+        pltpu.make_async_copy(refs[i], refs[count + i], sem.at[i]) for i in range(count)
+    ]
+    for copy in copies:
+        copy.start()
+    for copy in copies:
+        copy.wait()
+
+
+def stored(arrays):
+    return pl.pallas_call(
+        store_kernel,
+        out_shape=tuple(jax.ShapeDtypeStruct(x.shape, x.dtype) for x in arrays),
+        in_specs=[pl.BlockSpec(memory_space=pltpu.VMEM)] * len(arrays),
+        out_specs=[pl.BlockSpec(memory_space=pltpu.HBM)] * len(arrays),
+        scratch_shapes=[pltpu.SemaphoreType.DMA((len(arrays),))],
+        compiler_params=pltpu.CompilerParams(vmem_limit_bytes=4 * 1024 * 1024),
+        name="store",
+    )(*arrays)
+
+
 def shards(tokens, routes, route_weight, norm_gain, gate_train, up_train, down_train):
-    gate_new, up_new, down_new, mixed = layer(
+    results = layer(
         lax.axis_size("grp"),
         lax.axis_size("fs_0"),
         lax.axis_size("tp"),
-        tokens,
         routes.T,
         route_weight.T,
         norm_gain[None, :],
+        tokens,
         gate_train[0],
         up_train[0],
         down_train[0].T,
     )
+    gate_new, up_new, down_new, mixed = stored(results)
     return (gate_new.T[None], up_new.T[None], down_new[None], mixed.T)
 
 

time: 209 us -> 200 us (0.957); the launches traced: 208 us -> 196 us
  local copies, waits for them, and re-layouts: 8.32 us -> 0.68 us
  Pallas kernels: 199 us -> 195 us
    unnamed x18 -> x6, local copies, waits for them, and re-layouts: 8.32 us -> 0.68 us
    pallas_call x1, Pallas kernels: 199 us -> 194 us  [layer(): pl.pallas_call(functools.partial(layer_kernel, groups, chips, experts), o...]
where the time goes in v3:
time: 200 us; the launch traced here: 196 us
  Pallas kernels  195 us (98%)
    pallas_call x1, Pallas kernels, layer(): pl.pallas_call(functools.partial(layer_kernel, groups, chips, experts), o...  194 us

profile of v3, /device:TPU:41, one launch (start us, length us, event | category | flops | bytes accessed | tf_op | source)
XLA Modules:
  0.0 196.4 jit_solution(16822584175595664316)
XLA Ops:
  0.6 0.0 copy-start.1
  0.6 0.0 copy-start
  0.7 0.0 copy-start.2
  0.7 0.7 copy-done.1
  1.3 0.0 copy-done
  1.3 0.0 copy-done.2
  1.3 193.7 %layer.1 = (bf16[176,2048]{1,0:T(8,128)(2,1)S(1)}, bf16[176,2048]{1,0:T(8,128)(2,1)S(1)}, bf16[176,2048]{1,0:T(8,128)(2,1)S(1)}, bf16[32,192]{1,0:T(8,128)(2,1)S(1)}) custom-call(s32[2,192]{1,0:T(2,128)S(1)} %bitcast.16, f32[2,192]{1,0:T(2,128)S(1)} %bitcast.17, f32[1,32]{1,0:T(1,128)S(1)} %bitcast.18, bf16[192,2048]{1,0:T(8,128)(2,1)} %tokens_far.1, ...), custom_call_target="tpu_custom_call" | custom-call | tf_op jit(solution)/shard_map/layer/pallas_call | solution.py:574
  195.0 1.4 store.1
Async XLA Ops:
  0.6 0.7 copy-start.1
  0.6 0.7 copy-start
  0.7 0.7 copy-start.2

commit v4 on v3

--- a/solution.py
+++ b/solution.py
@@ -39,13 +39,10 @@
     select,
     outgoing,
     arrived,
-    turned,
-    picked,
     split_down,
     my_down,
     hidden_all,
     partial,
-    partial_in,
     column_out,
     returned,
     quad_send,
@@ -96,14 +93,20 @@
     def own_quad(j):
         return spread * (2 * j + parity) + g // 2
 
-    stride = blocks // own_count
-
-    def turn_of(other):
-        return lax.rem(other // spread // 2, own_count) * stride
-
-    def expected_quad(n):
-        place_in_list = lax.rem(my_block, blocks) // stride
-        return own_quad(lax.rem(place_in_list - n + own_count, own_count))
+    def listed(m, n):
+        if m == 1:
+            return jnp.where(lax.rem(q // (2 * spread), 2) == 1, blocks - 1 - n, n)
+        return n
+
+    def expected_quad(m, n):
+        if m == 1 and own_count > 1:
+            early = lax.rem(my_block, blocks) >= blocks // 2
+            wanted = own_count // 2
+            first_half = n < wanted
+            odd_turn = jnp.logical_xor(early, jnp.logical_not(first_half))
+            within = jnp.where(first_half, n, n - wanted)
+            return own_quad(2 * within + jnp.where(odd_turn, 1, 0))
+        return own_quad(n)
 
     def sender_of(other):
         right = lax.rem(z - (2 * other + 1) + chips, chips) < half_ring
@@ -158,7 +161,8 @@
     for step in range(1, groups):
         greet_device({"grp": lax.rem(g + step, groups)})
     for step in range(1, experts):
-        greet_device({"tp": lax.rem(t + step, experts)})
+        for core in range(2):
+            greet_device({"tp": lax.rem(t + step, experts), "fs_1": core})
     greet_device(at(next_chip, c))
     greet_device(at(last_chip, c))
 
@@ -173,7 +177,7 @@
     low[2, :, :] = full[2].astype(jnp.bfloat16)
 
     expected = jnp.where(active, blocks - jnp.where(own, 1, 0), 0)
-    pl.semaphore_wait(barrier, expected + groups - 1 + 3 + experts - 1 + 2)
+    pl.semaphore_wait(barrier, expected + groups - 1 + 3 + 2 * (experts - 1) + 2)
 
     def lanes_for(core):
         return pl.ds(pl.multiple_of((2 * half + core) * share, LANES), share)
@@ -201,7 +205,7 @@
         )
 
     def group_copy(m, j, step):
-        other = expected_quad(j)
+        other = expected_quad(m, j)
         return pltpu.make_async_remote_copy(
             src_ref=outputs[m].at[:, place(other)],
             dst_ref=outputs[m].at[:, place(other)],
@@ -303,7 +307,7 @@
             tile_buf[m, :, :] = rows_buf[m, :, :].T
 
             def send(n, _):
-                i = lax.rem(n + turn_of(q), blocks)
+                i = listed(m, n)
                 mine = is_mine(i)
 
                 @pl.when(mine)
@@ -319,37 +323,15 @@
             lax.fori_loop(0, blocks, send, 0)
 
 
-    chunk = 4 * LANES
-
-    def turn(k, _):
-        lanes = pl.ds(pl.multiple_of(k * chunk, chunk), chunk)
-        tall = jnp.concatenate(
-            [full[2, :, lanes], jnp.zeros((LANES - rows, chunk), jnp.float32)], axis=0
-        )
-        turned[lanes, :] = tall.T.astype(jnp.bfloat16)
-        return 0
-
-    lax.fori_loop(0, hidden // chunk, turn, 0)
-
-    def pick(k, _):
+    for k in range(half_ring):
         for p in range(2):
-            picked[p, block_rows(k), :] = turned[block_rows(2 * k + p), :]
-        return 0
-
-    lax.fori_loop(0, half_ring, pick, 0)
-    piece = 2 * LANES
-
-    def lay(k, _):
-        span = pl.ds(pl.multiple_of(k * piece, piece), piece)
-        for p in range(2):
-            split_down[p, :, span] = picked[p, span, :].T[:rows, :]
-        return 0
-
-    lax.fori_loop(0, hidden // 2 // piece, lay, 0)
-    my_down[rows_at(c), :] = split_down[c]
+            start = (2 * k + p) * units
+            split_down[p, k, :, :] = low[2, :, start : start + units]
+    for k in range(half_ring):
+        my_down[k, rows_at(c), :] = split_down[c, k]
     columns_copy = pltpu.make_async_remote_copy(
         src_ref=split_down.at[1 - c],
-        dst_ref=my_down.at[rows_at(c), :],
+        dst_ref=my_down.at[:, rows_at(c), :],
         send_sem=core_send.at[0],
         recv_sem=core_recv.at[0],
         device_id=at(z, 1 - c),
@@ -358,7 +340,7 @@
     columns_copy.start()
 
     def forward(m, j):
-        other = expected_quad(j)
+        other = expected_quad(m, j)
 
         @pl.when(jnp.logical_not(jnp.logical_and(own, other == q)))
         def _():
@@ -395,16 +377,13 @@
 
     wide = slots // 2
 
-    def hide(k, _):
-        own_tokens = arrived[pl.ds(k * (experts // 2), experts // 2)].reshape(wide, width)
+    def hide(k):
+        own_tokens = arrived[k * (experts // 2) : (k + 1) * (experts // 2)].reshape(wide, width)
         gated = lax.dot_general(gate_out[...], own_tokens, NT, preferred_element_type=jnp.float32)
         lifted = lax.dot_general(up_out[...], own_tokens, NT, preferred_element_type=jnp.float32)
         hidden_all[k, block_rows(pair), :] = (
             gated * (1.0 / (1.0 + jnp.exp(-gated))) * lifted
         ).astype(jnp.bfloat16)
-        return 0
-
-    lax.fori_loop(0, 2, hide, 0)
 
     part = wide // SUB
 
@@ -430,10 +409,23 @@
             device_id_type=MESH,
         )
 
+    def add_block(k, chip, fresh=False):
+        term = jnp.dot(
+            my_down[chip], hidden_all[k, block_rows(chip), :], preferred_element_type=jnp.float32
+        )
+        partial[k, :, :] = term if fresh else partial[k, :, :] + term
+
     for k in range(2):
+        hide(k)
         for j in range(SUB):
             for way in range(2):
                 hop_copy(way, k, 0, j).start()
+    columns_copy.wait()
+    for k in range(2):
+        add_block(k, pair, True)
+
+    def source_of(way, step):
+        return lax.rem(z + chips - step - 1 if way == 0 else z + step + 1, half_ring)
 
     def hop(step, _):
         @pl.when(step < own_count)
@@ -449,6 +441,9 @@
                     def _():
                         hop_copy(way, k, step + 1, j).start()
 
+        for k in range(2):
+            for way in range(2):
+                add_block(k, source_of(way, step))
         return 0
 
     lax.fori_loop(0, reach - 1, hop, 0)
@@ -457,64 +452,52 @@
     for way in range(2):
         for j in range(SUB):
             hop_arrival(way, way, reach - 1, j).wait_recv()
-    columns_copy.wait()
-
     for k in range(2):
-        partial[k, :, :] = jnp.dot(
-            my_down[...], hidden_all[k, :, :], preferred_element_type=jnp.float32
-        )
-
-    partial_copy = pltpu.make_async_remote_copy(
-        src_ref=partial.at[:, rows_at(1 - c), :],
-        dst_ref=partial_in,
-        send_sem=core_send.at[1],
-        recv_sem=core_recv.at[1],
-        device_id=at(z, 1 - c),
-        device_id_type=MESH,
-    )
-    partial_copy.start()
-    partial_copy.wait_recv()
+        add_block(k, source_of(k, reach - 1))
+
+    def back_copy(step, core):
+        other = lax.rem(t + step, experts)
+        return pltpu.make_async_remote_copy(
+            src_ref=column_out.at[other, rows_at(core), :],
+            dst_ref=returned.at[t, c],
+            send_sem=back_send.at[step, core],
+            recv_sem=back_recv.at[t, c],
+            device_id={"tp": other, "fs_1": core},
+            device_id_type=MESH,
+        )
+
+    def back_arrival(step, core):
+        other = lax.rem(t + step, experts)
+        return pltpu.make_async_remote_copy(
+            src_ref=column_out.at[other, rows_at(c), :],
+            dst_ref=returned.at[other, core],
+            send_sem=back_send.at[step, core],
+            recv_sem=back_recv.at[other, core],
+            device_id={"tp": other, "fs_1": core},
+            device_id_type=MESH,
+        )
+
     for e in range(experts):
         k, lane = e // (experts // 2), (e % (experts // 2)) * CAP
-        lanes = pl.ds(lane, CAP)
-        column_out[e, :, :] = (
-            partial[k, rows_at(c), lanes] + partial_in[k, :, lanes]
-        ).astype(jnp.bfloat16)
-
-    def back_copy(step):
-        other = lax.rem(t + step, experts)
-        return pltpu.make_async_remote_copy(
-            src_ref=column_out.at[other],
-            dst_ref=returned.at[t],
-            send_sem=back_send.at[step - 1],
-            recv_sem=back_recv.at[t],
-            device_id={"tp": other},
-            device_id_type=MESH,
-        )
-
-    def back_arrival(step):
-        other = lax.rem(t + step, experts)
-        return pltpu.make_async_remote_copy(
-            src_ref=column_out.at[other],
-            dst_ref=returned.at[other],
-            send_sem=back_send.at[step - 1],
-            recv_sem=back_recv.at[other],
-            device_id={"tp": other},
-            device_id_type=MESH,
-        )
-
+        column_out[e, :, :] = partial[k, :, lane : lane + CAP]
     for step in range(1, experts):
-        back_copy(step).start()
-    returned[t] = column_out[t]
+        for core in range(2):
+            back_copy(step, core).start()
+    back_copy(0, 1 - c).start()
+    returned[t, c] = column_out[t, rows_at(c), :]
+    back_arrival(0, 1 - c).wait_recv()
     for step in range(1, experts):
-        back_arrival(step).wait_recv()
+        for core in range(2):
+            back_arrival(step, core).wait_recv()
     total = jnp.zeros((rows, token_count), jnp.float32)
     for e in range(experts):
         weight = jnp.where(first == e, route_weight[0:1, :], 0.0) + jnp.where(
             second == e, route_weight[1:2, :], 0.0
         )
         total = total + weight * jnp.dot(
-            returned[e, :, :], select[e, :, :], preferred_element_type=jnp.float32
+            (returned[e, 0] + returned[e, 1]).astype(jnp.bfloat16),
+            select[e, :, :],
+            preferred_element_type=jnp.float32,
         )
     mixed_out[...] = total.astype(jnp.bfloat16)
 
@@ -554,10 +537,11 @@
         return 0
 
     lax.fori_loop(0, reach, hopped, 0)
-    partial_copy.wait_send()
     for step in range(1, experts):
         token_copy(step).wait_send()
-        back_copy(step).wait_send()
+        for core in range(2):
+            back_copy(step, core).wait_send()
+    back_copy(0, 1 - c).wait_send()
 
 
 def layer(groups, chips, experts, *operands):
@@ -591,15 +575,12 @@
             pltpu.VMEM((experts, CAP, tokens.shape[0]), jnp.bfloat16),
             pltpu.VMEM((experts, CAP, width), jnp.bfloat16),
             pltpu.VMEM((experts, CAP, width), jnp.bfloat16),
-            pltpu.VMEM((hidden, LANES), jnp.bfloat16),
-            pltpu.VMEM((2, hidden // 2, LANES), jnp.bfloat16),
-            pltpu.VMEM((2, rows, hidden // 2), jnp.bfloat16),
-            pltpu.VMEM((2 * rows, hidden // 2), jnp.bfloat16),
+            pltpu.VMEM((2, chips // 2, rows, units), jnp.bfloat16),
+            pltpu.VMEM((chips // 2, 2 * rows, units), jnp.bfloat16),
             pltpu.VMEM((2, hidden // 2, wide), jnp.bfloat16),
             pltpu.VMEM((2, 2 * rows, wide), jnp.float32),
-            pltpu.VMEM((2, rows, wide), jnp.float32),
-            pltpu.VMEM((experts, rows, CAP), jnp.bfloat16),
-            pltpu.VMEM((experts, rows, CAP), jnp.bfloat16),
+            pltpu.VMEM((experts, 2 * rows, CAP), jnp.float32),
+            pltpu.VMEM((experts, 2, rows, CAP), jnp.float32),
             dma((3, 3)),
             dma((3, 4)),
             dma((3, share // units)),
@@ -607,12 +588,12 @@
             dma((3, quads // groups, groups - 1)),
             dma((experts - 1,)),
             dma((experts,)),
-            dma((2,)),
-            dma((2,)),
+            dma((1,)),
+            dma((1,)),
             dma((2, 2, reach, SUB)),
             dma((2, 2, reach, SUB)),
-            dma((experts - 1,)),
-            dma((experts,)),
+            dma((experts, 2)),
+            dma((experts, 2)),
             dma((4,)),
         ],
         compiler_params=pltpu.CompilerParams(

time: 200 us -> 196 us (0.980)
  Pallas kernels: 195 us -> 192 us
    pallas_call x1, Pallas kernels: 194 us -> 191 us  [layer(): pl.pallas_call(functools.partial(layer_kernel, groups, chips, experts), o...]
where the time goes in v4:
time: 196 us; the launch traced here: 194 us
  Pallas kernels  192 us (98%)
    pallas_call x1, Pallas kernels, layer(): pl.pallas_call(functools.partial(layer_kernel, groups, chips, experts), o...  191 us

profile of v4, /device:TPU:41, one launch (start us, length us, event | category | flops | bytes accessed | tf_op | source)
XLA Modules:
  0.0 193.8 jit_solution(3091216398705047307)
XLA Ops:
  0.6 0.0 copy-start.1
  0.6 0.0 copy-start
  0.7 0.0 copy-start.2
  0.7 0.7 copy-done.1
  1.3 0.0 copy-done
  1.3 0.0 copy-done.2
  1.3 191.1 %layer.1 = (bf16[176,2048]{1,0:T(8,128)(2,1)S(1)}, bf16[176,2048]{1,0:T(8,128)(2,1)S(1)}, bf16[176,2048]{1,0:T(8,128)(2,1)S(1)}, bf16[32,192]{1,0:T(8,128)(2,1)S(1)}) custom-call(s32[2,192]{1,0:T(2,128)S(1)} %bitcast.16, f32[2,192]{1,0:T(2,128)S(1)} %bitcast.17, f32[1,32]{1,0:T(1,128)S(1)} %bitcast.18, bf16[192,2048]{1,0:T(8,128)(2,1)} %tokens_far.1, ...), custom_call_target="tpu_custom_call" | custom-call | tf_op jit(solution)/shard_map/layer/pallas_call | solution.py:558
  192.4 1.4 store.1
Async XLA Ops:
  0.6 0.7 copy-start.1
  0.6 0.7 copy-start
  0.7 0.7 copy-start.2

commit v5 on v4

--- a/solution.py
+++ b/solution.py
@@ -59,6 +59,7 @@
     back_send,
     back_recv,
     read_sem,
+    ready,
 ):
     g = lax.axis_index("grp")
     z = lax.axis_index("fs_0")
@@ -96,7 +97,7 @@
     def listed(m, n):
         if m == 1:
             return jnp.where(lax.rem(q // (2 * spread), 2) == 1, blocks - 1 - n, n)
-        return n
+        return lax.rem(n + c * (blocks // 2), blocks)
 
     def expected_quad(m, n):
         if m == 1 and own_count > 1:
@@ -108,10 +109,6 @@
             return own_quad(2 * within + jnp.where(odd_turn, 1, 0))
         return own_quad(n)
 
-    def sender_of(other):
-        right = lax.rem(z - (2 * other + 1) + chips, chips) < half_ring
-        return 2 * other + jnp.where(right, 1, 0)
-
     def target(i):
         chip = half * blocks + c * (blocks // 2) + i // 2
         right = lax.rem(chip - z + 2 * chips, half_ring)
@@ -145,17 +142,13 @@
     def greet_device(where):
         pl.semaphore_signal(barrier, inc=1, device_id=where, device_id_type=MESH)
 
-    def greet(j, _):
-        other = own_quad(j)
-        chip = sender_of(other)
-
-        @pl.when(jnp.logical_not(jnp.logical_and(own, other == q)))
-        def _():
-            greet_device(at(chip, my_source_core))
-
-        return 0
-
-    lax.fori_loop(0, own_count, greet, 0)
+    for k in range(reach // 2):
+        for core in range(2):
+            greet_device(at(lax.rem(z + chips - (2 * k + 1 + odd), chips), core))
+            greet_device(at(lax.rem(z + 2 * k + 2 - odd, chips), core))
+    ahead = lax.rem(jnp.where(odd == 1, z + reach, z + chips - reach), chips)
+    behind = lax.rem(jnp.where(odd == 1, z + chips - reach, z + reach), chips)
+    greet_device(at(ahead, c))
     for chip, core in quad_mates:
         greet_device(at(chip, core))
     for step in range(1, groups):
@@ -176,8 +169,7 @@
     reads[2].wait()
     low[2, :, :] = full[2].astype(jnp.bfloat16)
 
-    expected = jnp.where(active, blocks - jnp.where(own, 1, 0), 0)
-    pl.semaphore_wait(barrier, expected + groups - 1 + 3 + 2 * (experts - 1) + 2)
+    pl.semaphore_wait(barrier, groups - 1 + 3 + 2 * (experts - 1) + 2 + 2 * reach + 1)
 
     def lanes_for(core):
         return pl.ds(pl.multiple_of((2 * half + core) * share, LANES), share)
@@ -225,9 +217,25 @@
             device_id_type=MESH,
         )
 
+    def is_near(i):
+        chip, _ = target(i)
+        away = lax.rem(jnp.where(odd == 1, chip - z, z - chip) + chips, chips)
+        return away <= reach
+
     def is_mine(i):
         chip, core = target(i)
         return jnp.logical_and(chip == z, core == c)
+
+    def send_tile(m, i):
+        mine = is_mine(i)
+
+        @pl.when(mine)
+        def _():
+            outputs[m][:, place(q)] = tile_buf[m, block_rows(i), :]
+
+        @pl.when(jnp.logical_not(mine))
+        def _():
+            ring_copy(m, i).start()
 
     def token_copy(step):
         other = lax.rem(t + step, experts)
@@ -256,6 +264,8 @@
         for m in range(3):
             for k in range(3):
                 mate_copy(m, k).start()
+
+    pl.semaphore_signal(ready, inc=1, device_id=at(behind, c), device_id_type=MESH)
 
     token_count, width = tokens.shape
     first = routes[0:1, :]
@@ -307,20 +317,23 @@
             tile_buf[m, :, :] = rows_buf[m, :, :].T
 
             def send(n, _):
-                i = listed(m, n)
-                mine = is_mine(i)
-
-                @pl.when(mine)
+                send_tile(m, listed(m, n))
+                return 0
+
+            def send_if(near, n, _):
+                @pl.when(is_near(n) == near)
                 def _():
-                    outputs[m][:, place(q)] = tile_buf[m, block_rows(i), :]
-
-                @pl.when(jnp.logical_not(mine))
-                def _():
-                    ring_copy(m, i).start()
+                    send_tile(m, n)
 
                 return 0
 
+            if m == 0:
+                pl.semaphore_wait(ready, 1)
             lax.fori_loop(0, blocks, send, 0)
+
+    @pl.when(jnp.logical_not(active))
+    def _():
+        pl.semaphore_wait(ready, 1)
 
 
     for k in range(half_ring):
@@ -595,6 +608,7 @@
             dma((experts, 2)),
             dma((experts, 2)),
             dma((4,)),
+            pltpu.SemaphoreType.REGULAR,
         ],
         compiler_params=pltpu.CompilerParams(
             collective_id=0, has_side_effects=True, vmem_limit_bytes=52736 * 1024

time: 196 us -> 191 us (0.974); the launches traced: 194 us -> 191 us
  Pallas kernels: 192 us -> 189 us
    pallas_call x1, Pallas kernels: 191 us -> 188 us  [layer(): pl.pallas_call(functools.partial(layer_kernel, groups, chips, experts), o...]
where the time goes in v5:
time: 191 us
  Pallas kernels  189 us (99%)
    pallas_call x1, Pallas kernels, layer(): pl.pallas_call(functools.partial(layer_kernel, groups, chips, experts), o...  188 us

profile of v5, /device:TPU:41, one launch (start us, length us, event | category | flops | bytes accessed | tf_op | source)
XLA Modules:
  0.0 190.8 jit_solution(4290676289778179550)
XLA Ops:
  0.6 0.0 copy-start.1
  0.6 0.0 copy-start
  0.7 0.0 copy-start.2
  0.7 0.7 copy-done.1
  1.3 0.0 copy-done
  1.3 0.0 copy-done.2
  1.3 188.1 %layer.1 = (bf16[176,2048]{1,0:T(8,128)(2,1)S(1)}, bf16[176,2048]{1,0:T(8,128)(2,1)S(1)}, bf16[176,2048]{1,0:T(8,128)(2,1)S(1)}, bf16[32,192]{1,0:T(8,128)(2,1)S(1)}) custom-call(s32[2,192]{1,0:T(2,128)S(1)} %bitcast.16, f32[2,192]{1,0:T(2,128)S(1)} %bitcast.17, f32[1,32]{1,0:T(1,128)S(1)} %bitcast.18, bf16[192,2048]{1,0:T(8,128)(2,1)} %tokens_far.1, ...), custom_call_target="tpu_custom_call" | custom-call | tf_op jit(solution)/shard_map/layer/pallas_call | solution.py:571
  189.4 1.4 store.1
Async XLA Ops:
  0.6 0.7 copy-start.1
  0.6 0.7 copy-start
  0.7 0.7 copy-start.2

commit v6 on v5

--- a/solution.py
+++ b/solution.py
@@ -261,7 +261,7 @@
 
     @pl.when(active)
     def _():
-        for m in range(3):
+        for m in range(2):
             for k in range(3):
                 mate_copy(m, k).start()
 
@@ -330,6 +330,9 @@
             if m == 0:
                 pl.semaphore_wait(ready, 1)
             lax.fori_loop(0, blocks, send, 0)
+            if m == 0:
+                for k in range(3):
+                    mate_copy(2, k).start()
 
     @pl.when(jnp.logical_not(active))
     def _():
@@ -441,18 +444,26 @@
         return lax.rem(z + chips - step - 1 if way == 0 else z + step + 1, half_ring)
 
     def hop(step, _):
-        @pl.when(step < own_count)
+        skipped = reach - 1 - (own_count + 1) // 2
+
+        @pl.when(step >= skipped)
         def _():
-            forward(2, step)
-
-        for k in range(2):
+            forward(2, 2 * (step - skipped))
+            if own_count > 1:
+                forward(2, 2 * (step - skipped) + 1)
+
+        for long in (True, False):
             for j in range(SUB):
                 for way in range(2):
+                    k = way if long else 1 - way
                     hop_arrival(way, k, step, j).wait_recv()
-
-                    @pl.when(jnp.logical_or(step < reach - 2, k == way))
-                    def _():
+                    if long:
                         hop_copy(way, k, step + 1, j).start()
+                    else:
+
+                        @pl.when(step < reach - 2)
+                        def _():
+                            hop_copy(way, k, step + 1, j).start()
 
         for k in range(2):
             for way in range(2):
@@ -460,8 +471,6 @@
         return 0
 
     lax.fori_loop(0, reach - 1, hop, 0)
-    for j in range(reach - 1, own_count):
-        forward(2, j)
     for way in range(2):
         for j in range(SUB):
             hop_arrival(way, way, reach - 1, j).wait_recv()

time: 191 us -> 190 us (level)
  no operation moved by 1% of the time
where the time goes in v6:
time: 190 us; the launch traced here: 189 us
  Pallas kernels  188 us (99%)
    pallas_call x1, Pallas kernels, layer(): pl.pallas_call(functools.partial(layer_kernel, groups, chips, experts), o...  186 us

profile of v6, /device:TPU:41, one launch (start us, length us, event | category | flops | bytes accessed | tf_op | source)
XLA Modules:
  0.0 189.2 jit_solution(3113332326090956326)
XLA Ops:
  0.6 0.0 copy-start.1
  0.6 0.0 copy-start
  0.7 0.0 copy-start.2
  0.7 0.7 copy-done.1
  1.3 0.0 copy-done
  1.3 0.0 copy-done.2
  1.3 186.5 %layer.1 = (bf16[176,2048]{1,0:T(8,128)(2,1)S(1)}, bf16[176,2048]{1,0:T(8,128)(2,1)S(1)}, bf16[176,2048]{1,0:T(8,128)(2,1)S(1)}, bf16[32,192]{1,0:T(8,128)(2,1)S(1)}) custom-call(s32[2,192]{1,0:T(2,128)S(1)} %bitcast.16, f32[2,192]{1,0:T(2,128)S(1)} %bitcast.17, f32[1,32]{1,0:T(1,128)S(1)} %bitcast.18, bf16[192,2048]{1,0:T(8,128)(2,1)} %tokens_far.1, ...), custom_call_target="tpu_custom_call" | custom-call | tf_op jit(solution)/shard_map/layer/pallas_call | solution.py:580
  187.8 1.4 store.1
Async XLA Ops:
  0.6 0.7 copy-start.1
  0.6 0.7 copy-start
  0.7 0.7 copy-start.2
